TPU v7x, 32 devices: a whole 2x2x4 slice. The times are simulated.
32 devices in a mesh: sp: 4 (over z), fs: 4 (over y, x), tp: 2 (over core).
Axes of the slice: x: 2, y: 2, z: 4, core: 2. Of those that a mesh axis runs over, the one named last changes fastest.
Arguments:
- tokens: bfloat16 [4, 512, 2048], P('fs', 'sp'), may hold values from -6 to 6
- norm_gain: float32 [2048], replicated, may hold values from 0.1 to 1.9
- w_ret_query: bfloat16 [2048, 2048], P(('sp', 'fs'), 'tp'), may hold values from -0.125 to 0.125
- w_ret_key: bfloat16 [2048, 2048], P(('sp', 'fs'), 'tp'), may hold values from -0.125 to 0.125
- w_ret_value: bfloat16 [2048, 2048], P(('sp', 'fs'), 'tp'), may hold values from -0.125 to 0.125
- w_q_down: bfloat16 [2048, 768], P(('sp', 'fs'), 'tp'), may hold values from -0.125 to 0.125
- w_kv_down: bfloat16 [2048, 512], P(('sp', 'fs'), 'tp'), may hold values from -0.125 to 0.125
- w_rope_key: bfloat16 [2048, 64], P(('sp', 'fs')), may hold values from -0.125 to 0.125
- w_q_up: bfloat16 [768, 3072], P(None, 'tp'), may hold values from -0.21875 to 0.21875
- w_kv_up: bfloat16 [512, 4096], P(None, 'tp'), may hold values from -0.25 to 0.25
- q_lat_gain: float32 [768], replicated, may hold values from 0.4 to 10
- kv_lat_gain: float32 [512], replicated, may hold values from 0.4 to 10
- att_norm_gain: float32 [2048], P('tp'), may hold values from 0.1 to 1.9
- ret_norm_gain: float32 [2048], P('tp'), may hold values from 0.1 to 1.9
- w_ret_out: bfloat16 [2048, 2048], P(('sp', 'fs'), 'tp'), may hold values from -0.09375 to 0.09375
- w_att_out: bfloat16 [2048, 2048], P(('sp', 'fs'), 'tp'), may hold values from -0.09375 to 0.09375
- head_rate: float32 [8], P('tp'), may hold values from -0.05 to 0
- decay_shift: float32 [4, 8, 512], P('fs', 'tp', 'sp'), may hold values from -1.1 to 0
- start_state: float32 [4, 8, 256, 256], P('fs', 'tp'), may hold values from -20 to 20
Outputs:
- mixed: bfloat16 [4, 512, 2048], P('fs', ('sp', 'tp'))
All inputs are finite; a program needn't handle non-finite values.
Results may differ from a plain program's by a relative error of at most 0.018.
The roundings to bfloat16 on the way count: a program that leaves them out, or rounds other values in their place, can miss the bound.
Values may be sent and summed in bfloat16 or wider, within the bound.
A program may use at most 64 MiB of HBM per device.

v0:
```python
import functools

import numpy as np

import jax
import jax.numpy as jnp
from jax import lax
from jax.experimental import pallas as pl
from jax.experimental.pallas import tpu as pltpu
from jax.sharding import PartitionSpec as P

RET_DIM = 256
NOPE_DIM = 128
ROPE_DIM = 64
VAL_DIM = 128
KV_LAT = 512


EPSILON = 1e-06
THETA_BASE = 10000.0
TOP_PRECISION = lax.Precision.HIGHEST


def prefix(x, axis, combine, identity):
    peers, position = (lax.axis_size(axis), lax.axis_index(axis))
    everything = jax.tree.map(
        lambda part, kind: lax.all_gather(part.astype(kind), axis), x, (jnp.bfloat16, jnp.bfloat16)
    )
    start = jax.tree.map(
        lambda part, zero: jnp.broadcast_to(jnp.asarray(zero, part.dtype), part.shape), x, identity
    )

    def lap(k, before):
        reached = k < position
        new = combine(
            before, jax.tree.map(lambda part, own: part[k].astype(own.dtype), everything, x)
        )
        return jax.tree.map(lambda a, b: jnp.where(reached, a, b), new, before)

    return lax.fori_loop(0, peers, lap, start)


def angle_tables(positions, rot_width):
    half_width = rot_width // 2
    inverse = THETA_BASE ** (-jnp.arange(half_width, dtype=jnp.float32) * 2.0 / rot_width)
    angles = positions.astype(jnp.float32)[:, None] * inverse[None, :]
    return (jnp.cos(angles), jnp.sin(angles))


def rotate(values, cosine, sine):
    half_width = values.shape[-1] // 2
    front_half = values[..., :half_width]
    back_half = values[..., half_width:]
    return jnp.concatenate(
        [front_half * cosine - back_half * sine, back_half * cosine + front_half * sine], axis=-1
    )


def rms_scale(values, gain_vector):
    return (
        values
        * lax.rsqrt(jnp.mean(values * values, axis=-1, keepdims=True) + EPSILON)
        * gain_vector
    )


def chain_states(earlier, later):
    early_log, early_state = earlier
    late_log, late_state = later
    return (early_log + late_log, jnp.exp(late_log)[:, None, None] * early_state + late_state)


def rows_plan(
    tokens,
    norm_gain,
    w_ret_query,
    w_ret_key,
    w_ret_value,
    w_q_down,
    w_kv_down,
    w_rope_key,
    w_q_up,
    w_kv_up,
    q_lat_gain,
    kv_lat_gain,
    att_norm_gain,
    ret_norm_gain,
    w_ret_out,
    w_att_out,
    head_rate,
    decay_shift,
    start_state,
):
    tok_rows = tokens.shape[1]
    ret_local = head_rate.shape[0]
    att_local = w_q_up.shape[1] // (NOPE_DIM + ROPE_DIM)
    row_offset = lax.axis_index("sp") * tok_rows
    positions = row_offset + jnp.arange(tok_rows, dtype=jnp.int32)
    (
        full_query,
        full_key,
        full_value,
        full_q_down,
        full_kv_down,
        full_rope,
        full_ret_out,
        full_att_out,
    ) = (
        lax.all_gather(w_ret_query, ("sp", "fs"), axis=0, tiled=True),
        lax.all_gather(w_ret_key, ("sp", "fs"), axis=0, tiled=True),
        lax.all_gather(w_ret_value, ("sp", "fs"), axis=0, tiled=True),
        lax.all_gather(w_q_down, ("sp", "fs"), axis=0, tiled=True),
        lax.all_gather(w_kv_down, ("sp", "fs"), axis=0, tiled=True),
        lax.all_gather(w_rope_key, ("sp", "fs"), axis=0, tiled=True),
        lax.all_gather(w_ret_out, ("sp", "fs"), axis=0, tiled=True),
        lax.all_gather(w_att_out, ("sp", "fs"), axis=0, tiled=True),
    )
    source = tokens[0].astype(jnp.float32)
    normed = rms_scale(source, norm_gain).astype(jnp.bfloat16)
    ret_cos, ret_sin = angle_tables(positions, RET_DIM)
    rope_cos, rope_sin = angle_tables(positions, ROPE_DIM)

    def project(weight):
        return jnp.dot(normed, weight, preferred_element_type=jnp.float32)

    part_q = project(full_q_down).astype(jnp.bfloat16)
    part_kv = project(full_kv_down).astype(jnp.bfloat16)
    lat_q_raw, lat_kv_raw = (
        lax.all_gather(part_q, "tp", axis=1, tiled=True),
        lax.all_gather(part_kv, "tp", axis=1, tiled=True),
    )
    retention_query = rotate(
        project(full_query).reshape(tok_rows, ret_local, RET_DIM),
        ret_cos[:, None],
        ret_sin[:, None],
    ).astype(jnp.bfloat16)
    retention_key = (
        rotate(
            project(full_key).reshape(tok_rows, ret_local, RET_DIM),
            ret_cos[:, None],
            ret_sin[:, None],
        )
        * RET_DIM ** (-0.5)
    ).astype(jnp.bfloat16)
    retention_value = project(full_value).reshape(tok_rows, ret_local, RET_DIM).astype(jnp.bfloat16)
    rope_key = rotate(project(full_rope), rope_cos, rope_sin).astype(jnp.bfloat16)
    log_rates = head_rate[:, None] + decay_shift[0]
    cumul = jnp.cumsum(log_rates, axis=1)
    offsets = jnp.arange(tok_rows, dtype=jnp.int32)
    lower_mask = offsets[None, :] <= offsets[:, None]
    decay_matrix = jnp.exp(
        jnp.where(lower_mask[None], cumul[:, :, None] - cumul[:, None, :], -jnp.inf)
    )
    block_score_grid = (
        jnp.einsum(
            "zgq,ugq->gzu", retention_query, retention_key, preferred_element_type=jnp.float32
        )
        * decay_matrix
    ).astype(jnp.bfloat16)
    inside_block_output = jnp.einsum(
        "vzs,svp->zvp", block_score_grid, retention_value, preferred_element_type=jnp.float32
    )
    block_output_sum = cumul[:, -1]
    weighted_values = (
        retention_key.astype(jnp.float32) * jnp.exp(block_output_sum[:, None] - cumul).T[:, :, None]
    )
    contribution = jnp.einsum(
        "uzj,uzv->zjv",
        weighted_values,
        retention_value.astype(jnp.float32),
        precision=TOP_PRECISION,
    )
    identity = (jnp.zeros_like(block_output_sum), jnp.zeros_like(contribution))
    before_log, before_state = prefix(
        (block_output_sum, contribution), "sp", chain_states, identity
    )
    q_latent = rms_scale(lat_q_raw.astype(jnp.float32), q_lat_gain).astype(jnp.bfloat16)
    kv_latent = rms_scale(lat_kv_raw.astype(jnp.float32), kv_lat_gain).astype(jnp.bfloat16)
    query_full = jnp.dot(q_latent, w_q_up, preferred_element_type=jnp.float32).reshape(
        tok_rows, att_local, NOPE_DIM + ROPE_DIM
    )
    query_nope = query_full[..., :NOPE_DIM].astype(jnp.bfloat16)
    query_rope = rotate(query_full[..., NOPE_DIM:], rope_cos[:, None], rope_sin[:, None]).astype(
        jnp.bfloat16
    )
    att_scale = (NOPE_DIM + ROPE_DIM) ** (-0.5)

    def attend(carry, key_nope, key_values, key_rope, start):
        running_max, running_sum, running_acc = carry
        key_count = key_rope.shape[0]
        score_matrix = (
            jnp.einsum("qhd,khd->hqk", query_nope, key_nope, preferred_element_type=jnp.float32)
            + jnp.einsum("qhd,kd->hqk", query_rope, key_rope, preferred_element_type=jnp.float32)
        ) * att_scale
        key_positions = start + jnp.arange(key_count, dtype=jnp.int32)
        allowed = key_positions[None, :] <= positions[:, None]
        masked = jnp.where(allowed[None], score_matrix, -jnp.inf)
        new_max = jnp.maximum(running_max, jnp.max(masked, axis=-1))
        safe_max = jnp.where(jnp.isfinite(new_max), new_max, 0.0)
        weights = jnp.exp(masked - safe_max[..., None])
        rescale = jnp.exp(running_max - safe_max)
        new_sum = running_sum * rescale + jnp.sum(weights, axis=-1)
        new_acc = running_acc * rescale[..., None] + jnp.einsum(
            "hqk,khd->hqd",
            weights.astype(jnp.bfloat16),
            key_values,
            preferred_element_type=jnp.float32,
        )
        return (new_max, new_sum, new_acc)

    def expand_attend(carry_in, lat_piece, rope_piece, start):
        wide = (
            jnp.dot(lat_piece, w_kv_up, preferred_element_type=jnp.float32)
            .astype(jnp.bfloat16)
            .reshape(rope_piece.shape[0], att_local, NOPE_DIM + VAL_DIM)
        )
        return attend(carry_in, wide[..., :NOPE_DIM], wide[..., NOPE_DIM:], rope_piece, start)

    empty = (
        jnp.full((att_local, tok_rows), -jnp.inf, jnp.float32),
        jnp.zeros((att_local, tok_rows), jnp.float32),
        jnp.zeros((att_local, tok_rows, VAL_DIM), jnp.float32),
    )
    groups = lax.axis_size("tp")
    kv_part = KV_LAT // groups
    rope_part = ROPE_DIM // groups
    my_group = lax.axis_index("tp")
    joined = jnp.concatenate(
        [
            lax.dynamic_slice_in_dim(kv_latent, my_group * kv_part, kv_part, 1),
            lax.dynamic_slice_in_dim(rope_key, my_group * rope_part, rope_part, 1),
        ],
        axis=1,
    )
    all_rows = lax.all_gather(joined, "sp", axis=0, tiled=True)
    complete = lax.all_gather(all_rows, "tp", axis=1, tiled=True)
    total_rows = complete.shape[0]
    grouped = complete.reshape(total_rows, groups, kv_part + rope_part)
    lat_all = grouped[:, :, :kv_part].reshape(total_rows, KV_LAT)
    rope_all = grouped[:, :, kv_part:].reshape(total_rows, ROPE_DIM)

    def visit(block_index, carry_in):
        start = block_index * tok_rows
        lat_piece = lax.dynamic_slice_in_dim(lat_all, start, tok_rows, 0)
        rope_piece = lax.dynamic_slice_in_dim(rope_all, start, tok_rows, 0)
        return expand_attend(carry_in, lat_piece, rope_piece, start)

    final = lax.fori_loop(0, lax.axis_index("sp") + 1, visit, empty)
    att_raw = jnp.transpose(final[2] / final[1][..., None], (1, 0, 2))
    att_out = (
        rms_scale(att_raw, att_norm_gain.reshape(att_local, VAL_DIM))
        .astype(jnp.bfloat16)
        .reshape(tok_rows, att_local * VAL_DIM)
    )
    entering = jnp.exp(before_log)[:, None, None] * start_state[0] + before_state
    carried_term = (
        jnp.einsum(
            "nhd,hde->nhe", retention_query.astype(jnp.float32), entering, precision=TOP_PRECISION
        )
        * jnp.exp(cumul).T[:, :, None]
    )
    ret_raw = inside_block_output + carried_term
    row_mean = jnp.mean(ret_raw, axis=-1, keepdims=True)
    centered = ret_raw - row_mean
    row_var = jnp.mean(centered * centered, axis=-1, keepdims=True)
    ret_out = (
        (centered * lax.rsqrt(row_var + EPSILON) * ret_norm_gain.reshape(ret_local, RET_DIM))
        .astype(jnp.bfloat16)
        .reshape(tok_rows, ret_local * RET_DIM)
    )
    contract = (((1,), (1,)), ((), ()))
    mixed = lax.psum_scatter(
        (
            lax.dot_general(ret_out, full_ret_out, contract, preferred_element_type=jnp.float32)
            + lax.dot_general(att_out, full_att_out, contract, preferred_element_type=jnp.float32)
        ).astype(jnp.bfloat16),
        "tp",
        scatter_dimension=0,
        tiled=True,
    )
    return mixed[None]


MESH = pl.DeviceIdType.MESH
WIDE = RET_DIM
CONTRACT = (((1,), (1,)), ((), ()))
GROUPS = ((0, 2), (2, 2), (4, 1), (5, 1))
FIRST, LATER = (0, 1), (2, 3)


def heads_fit(mesh, ret_local, sequences, q_wide, kv_wide, up_wide):
    sizes = mesh.shape
    return (
        sizes["sp"] == 4
        and sizes["fs"] == 4
        and sizes["tp"] == 2
        and ret_local == sizes["sp"]
        and sequences == 1
        and up_wide == 2 * (NOPE_DIM + ROPE_DIM) * ret_local
        and q_wide % 128 == 0
        and kv_wide % 128 == 0
        and q_wide + kv_wide + 2 * ROPE_DIM <= ret_local * WIDE
    )


def wave_tables(length, wide):
    half_wide = wide // 2
    powers = np.arange(half_wide, dtype=np.float32) * np.float32(2.0 / wide)
    inverse = np.power(np.float32(THETA_BASE), -powers).astype(np.float32)
    angles = np.arange(length, dtype=np.float32)[:, None] * inverse[None, :]
    return np.cos(angles), np.sin(angles)


def three_parts(x):
    high = x.astype(jnp.bfloat16)
    rest = x - high.astype(jnp.float32)
    middle = rest.astype(jnp.bfloat16)
    low = (rest - middle.astype(jnp.float32)).astype(jnp.bfloat16)
    return high, middle, low


def layer_kernel(
    n_sp,
    q_wide,
    kv_wide,
    tok_ref,
    lat_ref,
    wq_ref,
    wk_ref,
    wv_ref,
    wr_ref,
    wa_ref,
    shift_ref,
    rate_ref,
    gain_ref,
    qgain_ref,
    kvgain_ref,
    again_ref,
    rgain_ref,
    rcos_ref,
    rsin_ref,
    pcos_ref,
    psin_ref,
    qup_ref,
    kvup_ref,
    start_ref,
    out_ref,
    tok_all,
    w_all,
    shift_all,
    normed,
    acc,
    ret_q,
    ret_k,
    ret_v,
    lat_all,
    state,
    qn,
    qr,
    expanded,
    rope_key,
    kvup,
    qup,
    merged,
    own_sum,
    pair_out,
    pair_in,
    row_out,
    row_in,
    local_sem,
    z_send,
    z_recv,
    x_send,
    x_recv,
    y_send,
    y_recv,
    f_send,
    f_recv,
    m_send,
    m_recv,
    l_send,
    l_recv,
    l_relay,
    p_send,
    p_recv,
):
    z, f, t = lax.axis_index("sp"), lax.axis_index("fs"), lax.axis_index("tp")
    xn = f + 1 - 2 * (f % 2)
    yn = (f + 2) % 4
    other = 1 - t
    fs = 4
    rows = tok_ref.shape[0]
    half = rows // 2
    weights = (lat_ref, wq_ref, wk_ref, wv_ref, wr_ref, wa_ref)
    f32, bf16 = jnp.float32, jnp.bfloat16

    def remote(src, dst, send, recv, **where):
        return pltpu.make_async_remote_copy(
            src_ref=src,
            dst_ref=dst,
            send_sem=send,
            recv_sem=recv,
            device_id={"sp": z, "fs": f, "tp": t, **where},
            device_id_type=MESH,
        )

    barrier = pltpu.get_barrier_semaphore()
    peers = [{"sp": (z + d) % n_sp, "fs": f, "tp": t} for d in range(1, n_sp)]
    peers += [{"sp": z, "fs": xn, "tp": t}, {"sp": z, "fs": yn, "tp": t}]
    peers += [{"sp": z, "fs": f, "tp": other}]
    for peer in peers:
        pl.semaphore_signal(barrier, inc=1, device_id=peer, device_id_type=MESH)
    pl.semaphore_wait(barrier, len(peers))

    def piece(u, owner):
        return weights[u].at[:, pl.ds(pl.multiple_of(owner * WIDE, WIDE), WIDE)]

    def part(owner_z, owner_f, g):
        first, count = GROUPS[g]
        start = pl.multiple_of((owner_z * fs + owner_f) * rows, rows)
        return w_all.at[pl.ds(start, rows), pl.ds(first * WIDE, count * WIDE)]

    def unit(u):
        start = pl.multiple_of((z * fs + f) * rows, rows)
        return w_all.at[pl.ds(start, rows), pl.ds(u * WIDE, WIDE)]

    pending = []

    def go(copy):
        copy.start()
        pending.append(copy)
        return copy

    def owner(d):
        return (z + n_sp - d) % n_sp

    mine = pl.ds(pl.multiple_of(t * half, half), half)
    z_copies, x_copies, y_copies, f_copies = {}, {}, {}, {}

    def tok_part(origin):
        return tok_all.at[origin, mine]

    def lat_part(i):
        return lambda origin: lat_all.at[t, origin, pl.ds(i * rows, rows)]

    def direct(dest):
        near = (z - dest == 1) | (dest - z == 1)
        return near if dest in (0, n_sp - 1) else z != dest

    def line_copy(where, row, dest, src=None):
        return remote(
            where(z) if src is None else src,
            where(z),
            l_send.at[row, dest],
            l_recv.at[row, z],
            sp=dest,
        )

    def relay_copy(where, row, origin, dest):
        ref = where(origin)
        return remote(ref, ref, l_relay.at[row, origin], l_recv.at[row, origin], sp=dest)

    def pair_copy(where, row, origin):
        ref = where(origin)
        return remote(ref, ref, p_send.at[row, origin], p_recv.at[row, origin], tp=other)

    def line_start(where, row, src=None, pair=True):
        for dest in range(n_sp):
            pl.when(direct(dest))(lambda dest=dest: line_copy(where, row, dest, src).start())
        if pair:
            for origin in range(n_sp):
                pl.when(origin == z)(
                    lambda origin=origin: pair_copy(where, row, origin).start()
                )

    def passes_on(origin):
        if origin < n_sp // 2:
            return z == n_sp - 2, n_sp - 1
        return z == 1, 0

    def line_pass(where, row):
        for origin in range(n_sp):

            @pl.when(origin != z)
            def _(origin=origin):
                relay_copy(where, row, origin, 0).wait_recv()
                should, dest = passes_on(origin)
                pl.when(should)(lambda: relay_copy(where, row, origin, dest).start())
                pair_copy(where, row, origin).start()

    def pair_arrive(where, row, own):
        for origin in range(n_sp):
            if own:
                pair_copy(where, row, origin).wait_recv()
            else:
                pl.when(origin != z)(
                    lambda origin=origin: pair_copy(where, row, origin).wait_recv()
                )

    def line_drain(where, row, own):
        for other_z in range(n_sp):
            pl.when(direct(other_z))(
                lambda dest=other_z: line_copy(where, row, dest).wait_send()
            )
            if own:
                pair_copy(where, row, other_z).wait_send()

            @pl.when(other_z != z)
            def _(origin=other_z):
                should, dest = passes_on(origin)
                pl.when(should)(lambda: relay_copy(where, row, origin, dest).wait_send())
                if not own:
                    pair_copy(where, row, origin).wait_send()

    line_start(tok_part, 0, tok_ref.at[mine], pair=False)
    for d in range(1, n_sp):
        to = (z + d) % n_sp
        go(remote(shift_ref, shift_all.at[z], m_send.at[2, d], m_recv.at[2, d], sp=to))
    shift_copies = list(pending)
    pending.clear()
    locals_ = []
    for u in range(6):
        copy = pltpu.make_async_copy(piece(u, z), unit(u), local_sem.at[u])
        copy.start()
        locals_.append(copy)
    own_tok = pltpu.make_async_copy(tok_ref, tok_all.at[z], local_sem.at[6])
    own_tok.start()
    own_shift = pltpu.make_async_copy(shift_ref, shift_all.at[z], local_sem.at[7])
    own_shift.start()
    att_wide = kvup.shape[1]
    own_kvup = pltpu.make_async_copy(
        kvup_ref.at[:, pl.ds(pl.multiple_of(z * att_wide, att_wide), att_wide)],
        kvup,
        local_sem.at[8],
    )
    own_kvup.start()
    up_wide = qup.shape[1]
    own_qup = pltpu.make_async_copy(
        qup_ref.at[:, pl.ds(pl.multiple_of(z * up_wide, up_wide), up_wide)],
        qup,
        local_sem.at[10],
    )
    own_qup.start()
    own_state = pltpu.make_async_copy(start_ref.at[z], state, local_sem.at[9])
    own_state.start()
    for group in (FIRST, LATER):
        for d in range(1, n_sp):
            to = (z + d) % n_sp
            for g in group:
                for u in range(GROUPS[g][0], sum(GROUPS[g])):
                    z_copies[d, u] = remote(
                        piece(u, to), unit(u), z_send.at[d, u], z_recv.at[d, u], sp=to
                    )
                    z_copies[d, u].start()

    def spread(d, group):
        for g in group:
            for u in range(GROUPS[g][0], sum(GROUPS[g])):
                if d == 0:
                    locals_[u].wait()
                else:
                    z_copies[d, u].wait_recv()
            ref = part(owner(d), f, g)
            x_copies[d, g] = remote(ref, ref, x_send.at[d, g], x_recv.at[d, g], fs=xn)
            y_copies[d, g] = remote(ref, ref, y_send.at[d, g], y_recv.at[d, g], fs=yn)
            x_copies[d, g].start()
            y_copies[d, g].start()

    def relay(d, group):
        for g in group:
            if g % 2 == 0:
                x_copies[d, g].wait_recv()
                ref, to = part(owner(d), xn, g), yn
            else:
                y_copies[d, g].wait_recv()
                ref, to = part(owner(d), yn, g), xn
            f_copies[d, g] = remote(ref, ref, f_send.at[d, g], f_recv.at[d, g], fs=to)
            f_copies[d, g].start()

    def arrive(d, group):
        for g in group:
            if g % 2 == 0:
                y_copies[d, g].wait_recv()
            else:
                x_copies[d, g].wait_recv()
            f_copies[d, g].wait_recv()

    def at(i):
        if isinstance(i, int):
            return slice(i * rows, (i + 1) * rows)
        return pl.ds(pl.multiple_of(i * rows, rows), rows)

    def norm_block(i):
        x = tok_all[i].astype(f32)
        scaled = x * lax.rsqrt(jnp.mean(x * x, axis=-1, keepdims=True) + EPSILON)
        normed[at(i), :] = (scaled * gain_ref[...]).astype(bf16)

    spread(0, FIRST)
    own_tok.wait()
    norm_block(z)
    line_pass(tok_part, 0)
    for d in range(1, n_sp):
        spread(d, FIRST)
        relay(d - 1, FIRST)
        if d == 1:
            pair_arrive(tok_part, 0, False)
        norm_block(owner(d))
    relay(n_sp - 1, FIRST)
    spread(0, LATER)
    depth = fs * rows
    for d in range(n_sp):
        arrive(d, FIRST)
        begin = pl.multiple_of(owner(d) * depth, depth)

        def multiply(i, carry, d=d, begin=begin):
            columns = pl.ds(pl.multiple_of(i * WIDE, WIDE), WIDE)
            got = jnp.dot(
                normed[:, pl.ds(begin, depth)],
                w_all[pl.ds(begin, depth), columns],
                preferred_element_type=f32,
            )
            if d == 0:
                acc[:, columns] = got
            else:
                acc[:, columns] += got
            return carry

        lax.fori_loop(0, 4, multiply, 0)

    rope_index = (q_wide + kv_wide) // WIDE
    rope_lane = (q_wide + kv_wide) % WIDE
    rd = RET_DIM // 2

    def finish_lat(i, carry):
        raw = acc[at(i), :WIDE]
        pair = raw[:, rope_lane : rope_lane + 2 * ROPE_DIM]
        turned = pair * pcos_ref[at(i), :] + pltpu.roll(pair, ROPE_DIM, 1) * psin_ref[at(i), :]
        lane = lax.broadcasted_iota(jnp.int32, turned.shape, 1)
        turned = jnp.where(lane < ROPE_DIM, turned, pltpu.roll(turned, ROPE_DIM, 1))
        pieces = [raw[:, :rope_lane]] if rope_lane else []
        pieces.append(jnp.where(z == rope_index, turned, pair))
        if rope_lane + 2 * ROPE_DIM < WIDE:
            pieces.append(raw[:, rope_lane + 2 * ROPE_DIM :])
        lat_all[t, z, at(i), :] = jnp.concatenate(pieces, axis=1).astype(bf16)
        return carry

    for i in range(n_sp):
        finish_lat(i, 0)
        line_start(lat_part(i), i + 1)

    def finish_ret(i, carry):
        cosine, sine = rcos_ref[at(i), :], rsin_ref[at(i), :]
        for dst, base, factor in ((ret_q, WIDE, 1.0), (ret_k, 2 * WIDE, RET_DIM ** (-0.5))):
            a, b = acc[at(i), base : base + rd], acc[at(i), base + rd : base + WIDE]
            dst[at(i), :rd] = ((a * cosine - b * sine) * factor).astype(bf16)
            dst[at(i), rd:] = ((b * cosine + a * sine) * factor).astype(bf16)
        ret_v[at(i), :] = acc[at(i), 3 * WIDE :].astype(bf16)
        return carry

    lax.fori_loop(0, n_sp, finish_ret, 0)

    for copy in shift_copies:
        copy.wait()
    own_shift.wait()
    own_state.wait()
    r_iota = lax.broadcasted_iota(jnp.int32, (rows, rows), 0)
    c_iota = lax.broadcasted_iota(jnp.int32, (rows, rows), 1)

    def retention(b):
        rates = shift_all[b]
        pick = lax.broadcasted_iota(jnp.int32, rates.shape, 0) == z
        chosen = lax.broadcasted_iota(jnp.int32, rate_ref.shape, 1) == z
        rate = jnp.sum(jnp.where(chosen, rate_ref[...], 0.0), axis=1, keepdims=True)
        row = jnp.sum(jnp.where(pick, rates, 0.0), axis=0, keepdims=True) + rate
        column = jnp.sum(jnp.where(r_iota == c_iota, row, 0.0), axis=1, keepdims=True)
        c_col = jnp.sum(jnp.where(c_iota <= r_iota, row, 0.0), axis=1, keepdims=True)
        c_row = jnp.sum(jnp.where(r_iota <= c_iota, column, 0.0), axis=0, keepdims=True)
        last = jnp.sum(row, axis=1, keepdims=True)
        decay = jnp.exp(jnp.where(c_iota <= r_iota, c_col - c_row, -jnp.inf))
        block = slice(b * rows, (b + 1) * rows)
        q, k, v = ret_q[block, :], ret_k[block, :], ret_v[block, :]
        scores = lax.dot_general(q, k, CONTRACT, preferred_element_type=f32) * decay
        raw = jnp.dot(scores.astype(bf16), v, preferred_element_type=f32)
        carried = sum(
            jnp.dot(q, s, preferred_element_type=f32) for s in three_parts(state[...])
        )
        raw = raw + carried * jnp.exp(c_col)
        if b < n_sp - 1:
            weighted = k.astype(f32) * jnp.exp(last - c_col)
            added = sum(
                lax.dot_general(w, v, (((0,), (0,)), ((), ())), preferred_element_type=f32)
                for w in three_parts(weighted)
            )
            state[...] = jnp.exp(last) * state[...] + added
        centered = raw - jnp.mean(raw, axis=-1, keepdims=True)
        variance = jnp.mean(centered * centered, axis=-1, keepdims=True)
        merged[block, :WIDE] = (centered * lax.rsqrt(variance + EPSILON) * rgain_ref[z]).astype(
            bf16
        )

    for b in range(n_sp):
        if b:
            spread(b, LATER)
            relay(b - 1, LATER)
        line_pass(lat_part(b), b + 1)
        retention(b)
    relay(n_sp - 1, LATER)
    own_kvup.wait()
    own_qup.wait()

    def chunks(first, count):
        found = []
        for core in range(2):
            for j in range(count // 128):
                lane = first + j * 128
                found.append((core, lane // WIDE, lane % WIDE))
        return found

    q_chunks, kv_chunks = chunks(0, q_wide), chunks(q_wide, kv_wide)
    rope_at = (rope_index, rope_lane)
    att_heads = att_wide // (NOPE_DIM + VAL_DIM)
    nope = att_heads * NOPE_DIM
    turn = att_heads * ROPE_DIM

    def expand(i, carry):
        def latent(found, gain):
            x = jnp.concatenate(
                [lat_all[c, s, at(i), lane : lane + 128] for c, s, lane in found], axis=1
            ).astype(f32)
            scaled = x * lax.rsqrt(jnp.mean(x * x, axis=-1, keepdims=True) + EPSILON)
            return (scaled * gain[...]).astype(bf16)

        query = jnp.dot(latent(q_chunks, qgain_ref), qup[...], preferred_element_type=f32)
        first, middle, end = query[:, :128], query[:, 128:256], query[:, 256:]
        lane = lax.broadcasted_iota(jnp.int32, first.shape, 1)
        second = jnp.where(
            lane < ROPE_DIM, pltpu.roll(middle, ROPE_DIM, 1), pltpu.roll(end, ROPE_DIM, 1)
        )
        pair = jnp.where(lane < ROPE_DIM, middle, end)
        quarter = ROPE_DIM // 2
        swapped = jnp.where(
            lane % ROPE_DIM < quarter,
            pltpu.roll(pair, 2 * ROPE_DIM - quarter, 1),
            pltpu.roll(pair, quarter, 1),
        )
        qn[at(i), :NOPE_DIM] = first.astype(bf16)
        qn[at(i), NOPE_DIM:] = second.astype(bf16)
        qr[at(i), :] = (pair * pcos_ref[at(i), :] + swapped * psin_ref[at(i), :]).astype(bf16)
        expanded[at(i), :] = jnp.dot(
            latent(kv_chunks, kvgain_ref), kvup[...], preferred_element_type=f32
        ).astype(bf16)
        rope_key[at(i), :] = lat_all[0, rope_at[0], at(i), rope_at[1] : rope_at[1] + 128]
        return carry

    for i in range(n_sp):
        pair_arrive(lat_part(i), i + 1, True)
        expand(i, 0)
    for d in range(n_sp):
        arrive(d, LATER)
    pair_copies = {}

    def row_copy(b, origin):
        return remote(row_out.at[b], row_in.at[origin], m_send.at[6, b], m_recv.at[6, origin], sp=b)

    def project_out(b):
        got = lax.dot_general(
            merged[b * rows : (b + 1) * rows, :],
            w_all[:, 4 * WIDE :],
            CONTRACT,
            preferred_element_type=f32,
        )
        front, back = got[:half, :], got[half:, :]
        pair_out[b] = jnp.where(t == 0, back, front).astype(bf16)
        pair_copies[b] = remote(
            pair_out.at[b], pair_in.at[b], m_send.at[5, b], m_recv.at[5, b], tp=other
        )
        pair_copies[b].start()
        own_sum[b] = jnp.where(t == 0, front, back)

    def send_rows(b):
        pair_copies[b].wait_recv()
        total = own_sum[b] + pair_in[b].astype(f32)
        own_sum[b] = total

        @pl.when(z != b)
        def _():
            row_out[b] = total.astype(bf16)
            row_copy(b, z).start()

    scale = (NOPE_DIM + ROPE_DIM) ** (-0.5)
    order = (0, n_sp - 1) + tuple(range(1, n_sp - 1))
    for step, b in enumerate(order):
        seen = (b + 1) * rows
        block = slice(b * rows, seen)
        q_at = lax.broadcasted_iota(jnp.int32, (rows, seen), 0) + b * rows
        k_at = lax.broadcasted_iota(jnp.int32, (rows, seen), 1)
        for h in range(att_heads):
            base = h * (NOPE_DIM + VAL_DIM)
            turned = qr[block, :]
            lane = lax.broadcasted_iota(jnp.int32, turned.shape, 1)
            turned = jnp.where(lane // ROPE_DIM == h, turned, jnp.zeros_like(turned))
            s = lax.dot_general(
                qn[block, h * NOPE_DIM : (h + 1) * NOPE_DIM],
                expanded[:seen, base : base + NOPE_DIM],
                CONTRACT,
                preferred_element_type=f32,
            ) + lax.dot_general(
                turned, rope_key[:seen, :], CONTRACT, preferred_element_type=f32
            )
            s = jnp.where(k_at <= q_at, s * scale, -jnp.inf)
            p = jnp.exp(s - jnp.max(s, axis=-1, keepdims=True))
            raw = jnp.dot(
                p.astype(bf16),
                expanded[:seen, base + NOPE_DIM : base + NOPE_DIM + VAL_DIM],
                preferred_element_type=f32,
            ) / jnp.sum(p, axis=-1, keepdims=True)
            scaled = raw * lax.rsqrt(jnp.mean(raw * raw, axis=-1, keepdims=True) + EPSILON)
            gain = again_ref[z][:, h * VAL_DIM : (h + 1) * VAL_DIM]
            merged[block, WIDE + h * VAL_DIM : WIDE + (h + 1) * VAL_DIM] = (
                scaled * gain
            ).astype(bf16)

        project_out(b)
        if step:
            send_rows(order[step - 1])
    send_rows(order[-1])
    total = own_sum[z]
    for d in range(1, n_sp):
        row_copy(0, owner(d)).wait_recv()
        total = total + row_in[owner(d)].astype(f32)
    out_ref[...] = total.astype(bf16)

    for group in (z_copies, x_copies, y_copies, f_copies, pair_copies):
        for copy in group.values():
            copy.wait_send()
    line_drain(tok_part, 0, False)
    for i in range(n_sp):
        line_drain(lat_part(i), i + 1, True)
    for b in range(n_sp):
        pl.when(z != b)(lambda b=b: row_copy(b, z).wait_send())


def heads_plan(
    tokens,
    norm_gain,
    w_ret_query,
    w_ret_key,
    w_ret_value,
    w_q_down,
    w_kv_down,
    w_rope_key,
    w_q_up,
    w_kv_up,
    q_lat_gain,
    kv_lat_gain,
    att_norm_gain,
    ret_norm_gain,
    w_ret_out,
    w_att_out,
    head_rate,
    decay_shift,
    start_state,
):
    n_sp = lax.axis_size("sp")
    rows, width = tokens.shape[1:]
    length = n_sp * rows
    q_wide, kv_wide = w_q_down.shape[1], w_kv_down.shape[1]
    rope_half = ROPE_DIM // 2
    w_rows = w_q_down.shape[0]
    att_heads = w_q_up.shape[1] // (NOPE_DIM + ROPE_DIM) // n_sp

    def swap(x):
        return jnp.concatenate([x[..., rope_half:], x[..., :rope_half]], axis=-1)

    lat = jnp.concatenate([w_q_down, w_kv_down, w_rope_key, swap(w_rope_key)], axis=1)
    lat = jnp.pad(lat, ((0, 0), (0, n_sp * WIDE - lat.shape[1])))
    ret_cos, ret_sin = wave_tables(length, RET_DIM)
    rope_cos, rope_sin = wave_tables(length, ROPE_DIM)
    pair_cos = np.concatenate([rope_cos] * 4, axis=1)
    pair_sin = np.concatenate([-rope_sin, rope_sin] * 2, axis=1)
    dma = pltpu.SemaphoreType.DMA
    vmem = pltpu.VMEM
    f32, bf16 = jnp.float32, jnp.bfloat16
    half = rows // 2
    out_wide = 4 * n_sp * w_rows
    any_spec = pl.BlockSpec(memory_space=pl.ANY)
    vmem_spec = pl.BlockSpec(memory_space=pltpu.VMEM)
    mixed = pl.pallas_call(
        functools.partial(layer_kernel, n_sp, q_wide, kv_wide),
        out_shape=jax.ShapeDtypeStruct((half, out_wide), bf16),
        in_specs=[any_spec] * 8 + [vmem_spec] * 10 + [any_spec] * 3,
        out_specs=vmem_spec,
        scratch_shapes=[
            vmem((n_sp, rows, width), bf16),
            vmem((n_sp * 4 * w_rows, 6 * WIDE), bf16),
            vmem((n_sp,) + decay_shift.shape[1:], f32),
            vmem((length, width), bf16),
            vmem((length, 4 * WIDE), f32),
            vmem((length, WIDE), bf16),
            vmem((length, WIDE), bf16),
            vmem((length, WIDE), bf16),
            vmem((2, n_sp, length, WIDE), bf16),
            vmem((RET_DIM, RET_DIM), f32),
            vmem((length, att_heads * NOPE_DIM), bf16),
            vmem((length, att_heads * ROPE_DIM), bf16),
            vmem((length, att_heads * (NOPE_DIM + VAL_DIM)), bf16),
            vmem((length, 2 * ROPE_DIM), bf16),
            vmem((w_kv_up.shape[0], att_heads * (NOPE_DIM + VAL_DIM)), bf16),
            vmem((w_q_up.shape[0], att_heads * (NOPE_DIM + ROPE_DIM)), bf16),
            vmem((length, WIDE + att_heads * VAL_DIM), bf16),
            vmem((n_sp, half, out_wide), f32),
            vmem((n_sp, half, out_wide), bf16),
            vmem((n_sp, half, out_wide), bf16),
            vmem((n_sp, half, out_wide), bf16),
            vmem((n_sp, half, out_wide), bf16),
            dma((11,)),
            dma((n_sp, 6)),
            dma((n_sp, 6)),
            dma((n_sp, 4)),
            dma((n_sp, 4)),
            dma((n_sp, 4)),
            dma((n_sp, 4)),
            dma((n_sp, 4)),
            dma((n_sp, 4)),
            dma((7, n_sp)),
            dma((7, n_sp)),
            dma((n_sp + 1, n_sp)),
            dma((n_sp + 1, n_sp)),
            dma((n_sp + 1, n_sp)),
            dma((n_sp + 1, n_sp)),
            dma((n_sp + 1, n_sp)),
        ],
        compiler_params=pltpu.CompilerParams(
            collective_id=0, has_side_effects=True, vmem_limit_bytes=62 * 1024 * 1024
        ),
    )(
        tokens[0],
        lat,
        w_ret_query,
        w_ret_key,
        w_ret_value,
        w_ret_out,
        w_att_out,
        decay_shift[0],
        head_rate[None],
        norm_gain[None],
        q_lat_gain[None],
        kv_lat_gain[None],
        att_norm_gain.reshape(n_sp, 1, -1),
        ret_norm_gain.reshape(n_sp, 1, -1),
        ret_cos,
        ret_sin,
        pair_cos,
        pair_sin,
        w_q_up,
        w_kv_up,
        start_state[0],
    )
    return mixed[None]


def solution(mesh):
    placed = (
        P("fs", "sp", None),
        P(),
        P(("sp", "fs"), "tp"),
        P(("sp", "fs"), "tp"),
        P(("sp", "fs"), "tp"),
        P(("sp", "fs"), "tp"),
        P(("sp", "fs"), "tp"),
        P(("sp", "fs"), None),
        P(None, "tp"),
        P(None, "tp"),
        P(),
        P(),
        P("tp"),
        P("tp"),
        P(("sp", "fs"), "tp"),
        P(("sp", "fs"), "tp"),
        P("tp"),
        P("fs", "tp", "sp"),
        P("fs", "tp", None, None),
    )

    def pick(*args):
        if heads_fit(
            mesh, args[16].shape[0], args[0].shape[0], args[5].shape[1], args[6].shape[1], args[8].shape[1]
        ):
            return heads_plan(*args)
        return rows_plan(*args)

    return jax.shard_map(
        pick,
        mesh=mesh,
        in_specs=placed,
        out_specs=P("fs", ("sp", "tp"), None),
        check_vma=False,
    )
```

profile of v0, /device:TPU:9, one launch (start us, length us, event | category | flops | bytes accessed | tf_op | source)
XLA Modules:
  0.0 132.7 jit_solution(10227294020020169801)
XLA Ops:
  0.0 1.3 broadcast_in_dim.17.qgain_ref
  1.3 0.8 copy.26
  2.1 0.1 fusion
  2.2 1.0 concatenate.3
  3.2 0.7 pad.4.lat_ref
  3.9 127.1 %shard_map.217 = bf16[64,2048]{1,0:T(8,128)(2,1)} custom-call(bf16[128,2048]{1,0:T(8,128)(2,1)} %bitcast.11, bf16[128,1024]{1,0:T(8,128)(2,1)} %pad.4.lat_ref, bf16[128,1024]{1,0:T(8,128)(2,1)} %wq_ref.1, bf16[128,1024]{1,0:T(8,128)(2,1)} %wk_ref.1, bf16[128,1024]{1,0:T(8,128)(2,1)} %wv_ref.1, bf16[128,1024]{1,0:T(8,128)(2,1)} %wr_ref.1, ...), custom_call_target="tpu_custom_call" | custom-call | tf_op jit(solution)/shard_map/pallas_call | solution.py:888
  131.1 1.7 %copy.28 = bf16[1,64,2048]{2,1,0:T(8,128)(2,1)} copy(bf16[1,64,2048]{2,1,0:T(8,128)(2,1)} %bitcast.10) | data formatting | bytes 524288
where the time goes:
time: 134 us; the launch traced here: 133 us
  Pallas kernels  127 us (95%)
  local copies, waits for them, and re-layouts  5.58 us (4%)
    pallas_call x1, Pallas kernels, heads_plan(): pl.pallas_call(functools.partial(layer_kernel, n_sp, q_wide, kv_wide), ou...  127 us

commit v1 on v0

--- a/solution.py
+++ b/solution.py
@@ -284,8 +284,9 @@
 MESH = pl.DeviceIdType.MESH
 WIDE = RET_DIM
 CONTRACT = (((1,), (1,)), ((), ()))
-GROUPS = ((0, 2), (2, 2), (4, 1), (5, 1))
-FIRST, LATER = (0, 1), (2, 3)
+UNITS = 6
+LAT, QUERY, KEY, VALUE, OUT_RET, OUT_ATT = range(UNITS)
+LAT_PARTS = 2
 
 
 def heads_fit(mesh, ret_local, sequences, q_wide, kv_wide, up_wide):
@@ -390,9 +391,12 @@
     other = 1 - t
     fs = 4
     rows = tok_ref.shape[0]
+    length = n_sp * rows
     half = rows // 2
     weights = (lat_ref, wq_ref, wk_ref, wv_ref, wr_ref, wa_ref)
     f32, bf16 = jnp.float32, jnp.bfloat16
+    lat_used = -(-(q_wide + kv_wide + 2 * ROPE_DIM) // WIDE)
+    others = range(1, n_sp)
 
     def remote(src, dst, send, recv, **where):
         return pltpu.make_async_remote_copy(
@@ -405,47 +409,114 @@
         )
 
     barrier = pltpu.get_barrier_semaphore()
-    peers = [{"sp": (z + d) % n_sp, "fs": f, "tp": t} for d in range(1, n_sp)]
+    peers = [{"sp": (z + d) % n_sp, "fs": f, "tp": t} for d in others]
     peers += [{"sp": z, "fs": xn, "tp": t}, {"sp": z, "fs": yn, "tp": t}]
     peers += [{"sp": z, "fs": f, "tp": other}]
     for peer in peers:
         pl.semaphore_signal(barrier, inc=1, device_id=peer, device_id_type=MESH)
-    pl.semaphore_wait(barrier, len(peers))
-
-    def piece(u, owner):
-        return weights[u].at[:, pl.ds(pl.multiple_of(owner * WIDE, WIDE), WIDE)]
-
-    def part(owner_z, owner_f, g):
-        first, count = GROUPS[g]
-        start = pl.multiple_of((owner_z * fs + owner_f) * rows, rows)
-        return w_all.at[pl.ds(start, rows), pl.ds(first * WIDE, count * WIDE)]
-
-    def unit(u):
-        start = pl.multiple_of((z * fs + f) * rows, rows)
-        return w_all.at[pl.ds(start, rows), pl.ds(u * WIDE, WIDE)]
-
-    pending = []
-
-    def go(copy):
-        copy.start()
-        pending.append(copy)
-        return copy
+    with jax.named_scope("barrier"):
+        pl.semaphore_wait(barrier, len(peers))
+
+    def at(i, size=rows):
+        if isinstance(i, int):
+            return slice(i * size, (i + 1) * size)
+        return pl.ds(pl.multiple_of(i * size, size), size)
 
     def owner(d):
         return (z + n_sp - d) % n_sp
 
+
+    def piece(u, dest):
+        return weights[u].at[:, at(dest, WIDE)]
+
+    def part(owner_z, owner_f, u):
+        return w_all.at[at(owner_z * fs + owner_f), u * WIDE : (u + 1) * WIDE]
+
+    def has(u, place):
+        return place < lat_used if u == LAT else True
+
+    def when(condition, action):
+        if condition is True:
+            action()
+        else:
+            pl.when(condition)(action)
+
+    def z_copy(d, u):
+        to = (z + d) % n_sp
+        return remote(piece(u, to), part(z, f, u), z_send.at[d, u], z_recv.at[d, u], sp=to)
+
+    def x_copy(d, u):
+        ref = part(owner(d), f, u)
+        return remote(ref, ref, x_send.at[d, u], x_recv.at[d, u], fs=xn)
+
+    def y_copy(d, u):
+        ref = part(owner(d), f, u)
+        return remote(ref, ref, y_send.at[d, u], y_recv.at[d, u], fs=yn)
+
+    def f_copy(d, u):
+        source, to = (xn, yn) if (d + u) % 2 == 0 else (yn, xn)
+        ref = part(owner(d), source, u)
+        return remote(ref, ref, f_send.at[d, u], f_recv.at[d, u], fs=to)
+
+    def own_copy(u):
+        return pltpu.make_async_copy(piece(u, z), part(z, f, u), local_sem.at[u])
+
+    def on_relay_link(to):
+        return ((z == 1) & (to == 0)) | ((z == n_sp - 2) & (to == n_sp - 1))
+
+    def send(units, held):
+        for u in units:
+            for d in others:
+                to = (z + d) % n_sp
+                condition = on_relay_link(to) if held else ~on_relay_link(to)
+                if u == LAT:
+                    condition = condition & has(u, to)
+                pl.when(condition)(lambda d=d, u=u: z_copy(d, u).start())
+
+    def spread(d, u):
+        def action():
+            with jax.named_scope(f"spread#d={d}#u={u}"):
+                if d == 0:
+                    own_copy(u).wait()
+                else:
+                    z_copy(d, u).wait_recv()
+            x_copy(d, u).start()
+            y_copy(d, u).start()
+
+        when(has(u, z), action)
+
+    def relay(d, u):
+        def action():
+            with jax.named_scope(f"relay#d={d}#u={u}"):
+                (x_copy if (d + u) % 2 == 0 else y_copy)(d, u).wait_recv()
+            f_copy(d, u).start()
+
+        when(has(u, z), action)
+
+    def arrive(d, u):
+        def action():
+            with jax.named_scope(f"arrive#d={d}#u={u}"):
+                (y_copy if (d + u) % 2 == 0 else x_copy)(d, u).wait_recv()
+                f_copy(d, u).wait_recv()
+
+        when(has(u, z), action)
+
+
     mine = pl.ds(pl.multiple_of(t * half, half), half)
-    z_copies, x_copies, y_copies, f_copies = {}, {}, {}, {}
 
     def tok_part(origin):
         return tok_all.at[origin, mine]
 
+    lat_rows = length // LAT_PARTS
+
     def lat_part(i):
-        return lambda origin: lat_all.at[t, origin, pl.ds(i * rows, rows)]
-
-    def direct(dest):
-        near = (z - dest == 1) | (dest - z == 1)
-        return near if dest in (0, n_sp - 1) else z != dest
+        return lambda origin: lat_all.at[t, origin, pl.ds(i * lat_rows, lat_rows)]
+
+    def sends(row, origin):
+        return True if row == 0 else origin < lat_used
+
+    def both(condition, more):
+        return condition if more is True else condition & more
 
     def line_copy(where, row, dest, src=None):
         return remote(
@@ -464,205 +535,167 @@
         ref = where(origin)
         return remote(ref, ref, p_send.at[row, origin], p_recv.at[row, origin], tp=other)
 
-    def line_start(where, row, src=None, pair=True):
+    def direct(dest):
+        near = (z - dest == 1) | (dest - z == 1)
+        return near if dest in (0, n_sp - 1) else z != dest
+
+    def line_start(where, row, src=None):
+        for distance in others:
+            for dest in range(n_sp):
+                condition = direct(dest) & ((z - dest == distance) | (dest - z == distance))
+                pl.when(both(condition, sends(row, z)))(
+                    lambda dest=dest: line_copy(where, row, dest, src).start()
+                )
+
+    ends = ((1, 0), (n_sp - 2, n_sp - 1))
+
+    def line_relay(where, row, distance):
+        for middle, dest in ends:
+            origin = middle + (middle - dest) * distance
+
+            @pl.when(both(z == middle, sends(row, origin)))
+            def _(origin=origin, dest=dest):
+                with jax.named_scope(f"line#r={row}#k={distance}"):
+                    relay_copy(where, row, origin, dest).wait_recv()
+                relay_copy(where, row, origin, dest).start()
+
+    def was_relayed(origin):
+        return z == (n_sp - 2 if origin < n_sp // 2 else 1)
+
+    def line_pair(where, row):
+        for distance in others:
+            for origin in range(n_sp):
+                here = (z - origin == distance) | (origin - z == distance)
+
+                @pl.when(both(here, sends(row, origin)))
+                def _(origin=origin):
+                    with jax.named_scope(f"pass#r={row}#k={distance}"):
+                        pl.when(~was_relayed(origin))(
+                            lambda: relay_copy(where, row, origin, 0).wait_recv()
+                        )
+                    pair_copy(where, row, origin).start()
+
+    def pair_own(where, row):
+        for origin in range(n_sp):
+            pl.when(both(origin == z, sends(row, origin)))(
+                lambda origin=origin: pair_copy(where, row, origin).start()
+            )
+
+    def pair_arrive(where, row, own):
+        with jax.named_scope(f"pair#r={row}"):
+            for origin in range(n_sp):
+                condition = sends(row, origin) if own else both(origin != z, sends(row, origin))
+                when(condition, lambda origin=origin: pair_copy(where, row, origin).wait_recv())
+
+    def line_drain(where, row, own):
         for dest in range(n_sp):
-            pl.when(direct(dest))(lambda dest=dest: line_copy(where, row, dest, src).start())
-        if pair:
-            for origin in range(n_sp):
-                pl.when(origin == z)(
-                    lambda origin=origin: pair_copy(where, row, origin).start()
+            pl.when(both(direct(dest), sends(row, z)))(
+                lambda dest=dest: line_copy(where, row, dest).wait_send()
+            )
+        for middle, dest in ends:
+            for distance in range(1, n_sp - 1):
+                origin = middle + (middle - dest) * distance
+                pl.when(both(z == middle, sends(row, origin)))(
+                    lambda origin=origin, dest=dest: relay_copy(
+                        where, row, origin, dest
+                    ).wait_send()
                 )
-
-    def passes_on(origin):
-        if origin < n_sp // 2:
-            return z == n_sp - 2, n_sp - 1
-        return z == 1, 0
-
-    def line_pass(where, row):
         for origin in range(n_sp):
-
-            @pl.when(origin != z)
-            def _(origin=origin):
-                relay_copy(where, row, origin, 0).wait_recv()
-                should, dest = passes_on(origin)
-                pl.when(should)(lambda: relay_copy(where, row, origin, dest).start())
-                pair_copy(where, row, origin).start()
-
-    def pair_arrive(where, row, own):
-        for origin in range(n_sp):
-            if own:
-                pair_copy(where, row, origin).wait_recv()
-            else:
-                pl.when(origin != z)(
-                    lambda origin=origin: pair_copy(where, row, origin).wait_recv()
-                )
-
-    def line_drain(where, row, own):
-        for other_z in range(n_sp):
-            pl.when(direct(other_z))(
-                lambda dest=other_z: line_copy(where, row, dest).wait_send()
-            )
-            if own:
-                pair_copy(where, row, other_z).wait_send()
-
-            @pl.when(other_z != z)
-            def _(origin=other_z):
-                should, dest = passes_on(origin)
-                pl.when(should)(lambda: relay_copy(where, row, origin, dest).wait_send())
-                if not own:
-                    pair_copy(where, row, origin).wait_send()
-
-    line_start(tok_part, 0, tok_ref.at[mine], pair=False)
-    for d in range(1, n_sp):
+            condition = sends(row, origin) if own else both(origin != z, sends(row, origin))
+            when(condition, lambda origin=origin: pair_copy(where, row, origin).wait_send())
+
+    def shift_copy(d):
         to = (z + d) % n_sp
-        go(remote(shift_ref, shift_all.at[z], m_send.at[2, d], m_recv.at[2, d], sp=to))
-    shift_copies = list(pending)
-    pending.clear()
-    locals_ = []
-    for u in range(6):
-        copy = pltpu.make_async_copy(piece(u, z), unit(u), local_sem.at[u])
-        copy.start()
-        locals_.append(copy)
+        return remote(shift_ref, shift_all.at[z], m_send.at[0, d], m_recv.at[0, d], sp=to)
+
+
+    line_start(tok_part, 0, tok_ref.at[mine])
+    for d in others:
+        shift_copy(d).start()
+    for u in range(UNITS):
+        when(has(u, z), lambda u=u: own_copy(u).start())
+    send((LAT,), True)
+    send((LAT, QUERY, KEY, VALUE), False)
     own_tok = pltpu.make_async_copy(tok_ref, tok_all.at[z], local_sem.at[6])
     own_tok.start()
     own_shift = pltpu.make_async_copy(shift_ref, shift_all.at[z], local_sem.at[7])
     own_shift.start()
     att_wide = kvup.shape[1]
-    own_kvup = pltpu.make_async_copy(
-        kvup_ref.at[:, pl.ds(pl.multiple_of(z * att_wide, att_wide), att_wide)],
-        kvup,
-        local_sem.at[8],
-    )
+    own_kvup = pltpu.make_async_copy(kvup_ref.at[:, at(z, att_wide)], kvup, local_sem.at[8])
     own_kvup.start()
     up_wide = qup.shape[1]
-    own_qup = pltpu.make_async_copy(
-        qup_ref.at[:, pl.ds(pl.multiple_of(z * up_wide, up_wide), up_wide)],
-        qup,
-        local_sem.at[10],
-    )
+    own_qup = pltpu.make_async_copy(qup_ref.at[:, at(z, up_wide)], qup, local_sem.at[10])
     own_qup.start()
     own_state = pltpu.make_async_copy(start_ref.at[z], state, local_sem.at[9])
     own_state.start()
-    for group in (FIRST, LATER):
-        for d in range(1, n_sp):
-            to = (z + d) % n_sp
-            for g in group:
-                for u in range(GROUPS[g][0], sum(GROUPS[g])):
-                    z_copies[d, u] = remote(
-                        piece(u, to), unit(u), z_send.at[d, u], z_recv.at[d, u], sp=to
-                    )
-                    z_copies[d, u].start()
-
-    def spread(d, group):
-        for g in group:
-            for u in range(GROUPS[g][0], sum(GROUPS[g])):
-                if d == 0:
-                    locals_[u].wait()
-                else:
-                    z_copies[d, u].wait_recv()
-            ref = part(owner(d), f, g)
-            x_copies[d, g] = remote(ref, ref, x_send.at[d, g], x_recv.at[d, g], fs=xn)
-            y_copies[d, g] = remote(ref, ref, y_send.at[d, g], y_recv.at[d, g], fs=yn)
-            x_copies[d, g].start()
-            y_copies[d, g].start()
-
-    def relay(d, group):
-        for g in group:
-            if g % 2 == 0:
-                x_copies[d, g].wait_recv()
-                ref, to = part(owner(d), xn, g), yn
-            else:
-                y_copies[d, g].wait_recv()
-                ref, to = part(owner(d), yn, g), xn
-            f_copies[d, g] = remote(ref, ref, f_send.at[d, g], f_recv.at[d, g], fs=to)
-            f_copies[d, g].start()
-
-    def arrive(d, group):
-        for g in group:
-            if g % 2 == 0:
-                y_copies[d, g].wait_recv()
-            else:
-                x_copies[d, g].wait_recv()
-            f_copies[d, g].wait_recv()
-
-    def at(i):
-        if isinstance(i, int):
-            return slice(i * rows, (i + 1) * rows)
-        return pl.ds(pl.multiple_of(i * rows, rows), rows)
 
     def norm_block(i):
         x = tok_all[i].astype(f32)
         scaled = x * lax.rsqrt(jnp.mean(x * x, axis=-1, keepdims=True) + EPSILON)
         normed[at(i), :] = (scaled * gain_ref[...]).astype(bf16)
 
-    spread(0, FIRST)
-    own_tok.wait()
-    norm_block(z)
-    line_pass(tok_part, 0)
-    for d in range(1, n_sp):
-        spread(d, FIRST)
-        relay(d - 1, FIRST)
-        if d == 1:
-            pair_arrive(tok_part, 0, False)
-        norm_block(owner(d))
-    relay(n_sp - 1, FIRST)
-    spread(0, LATER)
     depth = fs * rows
-    for d in range(n_sp):
-        arrive(d, FIRST)
-        begin = pl.multiple_of(owner(d) * depth, depth)
-
-        def multiply(i, carry, d=d, begin=begin):
-            columns = pl.ds(pl.multiple_of(i * WIDE, WIDE), WIDE)
-            got = jnp.dot(
-                normed[:, pl.ds(begin, depth)],
-                w_all[pl.ds(begin, depth), columns],
+
+    def multiply(u):
+        with jax.named_scope(f"multiply#u={u}"):
+            acc[...] = jnp.dot(
+                normed[:, :depth],
+                w_all[:depth, u * WIDE : (u + 1) * WIDE],
                 preferred_element_type=f32,
             )
-            if d == 0:
-                acc[:, columns] = got
-            else:
-                acc[:, columns] += got
-            return carry
-
-        lax.fori_loop(0, 4, multiply, 0)
+
+            def chunk(i, carry):
+                begin = at(i, depth)
+                acc[...] += jnp.dot(
+                    normed[:, begin],
+                    w_all[begin, u * WIDE : (u + 1) * WIDE],
+                    preferred_element_type=f32,
+                )
+                return carry
+
+            lax.fori_loop(1, n_sp, chunk, 0)
 
     rope_index = (q_wide + kv_wide) // WIDE
     rope_lane = (q_wide + kv_wide) % WIDE
     rd = RET_DIM // 2
 
-    def finish_lat(i, carry):
-        raw = acc[at(i), :WIDE]
-        pair = raw[:, rope_lane : rope_lane + 2 * ROPE_DIM]
-        turned = pair * pcos_ref[at(i), :] + pltpu.roll(pair, ROPE_DIM, 1) * psin_ref[at(i), :]
-        lane = lax.broadcasted_iota(jnp.int32, turned.shape, 1)
-        turned = jnp.where(lane < ROPE_DIM, turned, pltpu.roll(turned, ROPE_DIM, 1))
-        pieces = [raw[:, :rope_lane]] if rope_lane else []
-        pieces.append(jnp.where(z == rope_index, turned, pair))
-        if rope_lane + 2 * ROPE_DIM < WIDE:
-            pieces.append(raw[:, rope_lane + 2 * ROPE_DIM :])
-        lat_all[t, z, at(i), :] = jnp.concatenate(pieces, axis=1).astype(bf16)
-        return carry
-
-    for i in range(n_sp):
-        finish_lat(i, 0)
-        line_start(lat_part(i), i + 1)
-
-    def finish_ret(i, carry):
-        cosine, sine = rcos_ref[at(i), :], rsin_ref[at(i), :]
-        for dst, base, factor in ((ret_q, WIDE, 1.0), (ret_k, 2 * WIDE, RET_DIM ** (-0.5))):
-            a, b = acc[at(i), base : base + rd], acc[at(i), base + rd : base + WIDE]
+    def finish_lat():
+        def block(i, carry):
+            raw = acc[at(i), :]
+            pair = raw[:, rope_lane : rope_lane + 2 * ROPE_DIM]
+            turned = pair * pcos_ref[at(i), :] + pltpu.roll(pair, ROPE_DIM, 1) * psin_ref[at(i), :]
+            lane = lax.broadcasted_iota(jnp.int32, turned.shape, 1)
+            turned = jnp.where(lane < ROPE_DIM, turned, pltpu.roll(turned, ROPE_DIM, 1))
+            pieces = [raw[:, :rope_lane]] if rope_lane else []
+            pieces.append(jnp.where(z == rope_index, turned, pair))
+            if rope_lane + 2 * ROPE_DIM < WIDE:
+                pieces.append(raw[:, rope_lane + 2 * ROPE_DIM :])
+            lat_all[t, z, at(i), :] = jnp.concatenate(pieces, axis=1).astype(bf16)
+            return carry
+
+        lax.fori_loop(0, n_sp, block, 0)
+
+    def finish_turned(dst, factor):
+        def block(i, carry):
+            cosine, sine = rcos_ref[at(i), :], rsin_ref[at(i), :]
+            a, b = acc[at(i), :rd], acc[at(i), rd:]
             dst[at(i), :rd] = ((a * cosine - b * sine) * factor).astype(bf16)
             dst[at(i), rd:] = ((b * cosine + a * sine) * factor).astype(bf16)
-        ret_v[at(i), :] = acc[at(i), 3 * WIDE :].astype(bf16)
-        return carry
-
-    lax.fori_loop(0, n_sp, finish_ret, 0)
-
-    for copy in shift_copies:
-        copy.wait()
-    own_shift.wait()
-    own_state.wait()
+            return carry
+
+        lax.fori_loop(0, n_sp, block, 0)
+
+    def project(u):
+        for d in range(n_sp):
+            arrive(d, u)
+        multiply(u)
+        if u == QUERY:
+            finish_turned(ret_q, 1.0)
+        elif u == KEY:
+            finish_turned(ret_k, RET_DIM ** (-0.5))
+        else:
+            ret_v[...] = acc[...].astype(bf16)
+
     r_iota = lax.broadcasted_iota(jnp.int32, (rows, rows), 0)
     c_iota = lax.broadcasted_iota(jnp.int32, (rows, rows), 1)
 
@@ -698,16 +731,6 @@
             bf16
         )
 
-    for b in range(n_sp):
-        if b:
-            spread(b, LATER)
-            relay(b - 1, LATER)
-        line_pass(lat_part(b), b + 1)
-        retention(b)
-    relay(n_sp - 1, LATER)
-    own_kvup.wait()
-    own_qup.wait()
-
     def chunks(first, count):
         found = []
         for core in range(2):
@@ -719,10 +742,8 @@
     q_chunks, kv_chunks = chunks(0, q_wide), chunks(q_wide, kv_wide)
     rope_at = (rope_index, rope_lane)
     att_heads = att_wide // (NOPE_DIM + VAL_DIM)
-    nope = att_heads * NOPE_DIM
-    turn = att_heads * ROPE_DIM
-
-    def expand(i, carry):
+
+    def expand(i):
         def latent(found, gain):
             x = jnp.concatenate(
                 [lat_all[c, s, at(i), lane : lane + 128] for c, s, lane in found], axis=1
@@ -750,46 +771,10 @@
             latent(kv_chunks, kvgain_ref), kvup[...], preferred_element_type=f32
         ).astype(bf16)
         rope_key[at(i), :] = lat_all[0, rope_at[0], at(i), rope_at[1] : rope_at[1] + 128]
-        return carry
-
-    for i in range(n_sp):
-        pair_arrive(lat_part(i), i + 1, True)
-        expand(i, 0)
-    for d in range(n_sp):
-        arrive(d, LATER)
-    pair_copies = {}
-
-    def row_copy(b, origin):
-        return remote(row_out.at[b], row_in.at[origin], m_send.at[6, b], m_recv.at[6, origin], sp=b)
-
-    def project_out(b):
-        got = lax.dot_general(
-            merged[b * rows : (b + 1) * rows, :],
-            w_all[:, 4 * WIDE :],
-            CONTRACT,
-            preferred_element_type=f32,
-        )
-        front, back = got[:half, :], got[half:, :]
-        pair_out[b] = jnp.where(t == 0, back, front).astype(bf16)
-        pair_copies[b] = remote(
-            pair_out.at[b], pair_in.at[b], m_send.at[5, b], m_recv.at[5, b], tp=other
-        )
-        pair_copies[b].start()
-        own_sum[b] = jnp.where(t == 0, front, back)
-
-    def send_rows(b):
-        pair_copies[b].wait_recv()
-        total = own_sum[b] + pair_in[b].astype(f32)
-        own_sum[b] = total
-
-        @pl.when(z != b)
-        def _():
-            row_out[b] = total.astype(bf16)
-            row_copy(b, z).start()
 
     scale = (NOPE_DIM + ROPE_DIM) ** (-0.5)
-    order = (0, n_sp - 1) + tuple(range(1, n_sp - 1))
-    for step, b in enumerate(order):
+
+    def attend(b):
         seen = (b + 1) * rows
         block = slice(b * rows, seen)
         q_at = lax.broadcasted_iota(jnp.int32, (rows, seen), 0) + b * rows
@@ -820,23 +805,153 @@
                 scaled * gain
             ).astype(bf16)
 
-        project_out(b)
+    def out_copy(b):
+        return remote(pair_out.at[b], pair_in.at[b], m_send.at[1, b], m_recv.at[1, b], tp=other)
+
+    def row_copy(b, origin):
+        return remote(row_out.at[b], row_in.at[origin], m_send.at[2, b], m_recv.at[2, origin], sp=b)
+
+    def project_out(b):
+        got = lax.dot_general(
+            merged[at(b), :],
+            w_all[:, OUT_RET * WIDE :],
+            CONTRACT,
+            preferred_element_type=f32,
+        )
+        front, back = got[:half, :], got[half:, :]
+        pair_out[b] = jnp.where(t == 0, back, front).astype(bf16)
+        out_copy(b).start()
+        own_sum[b] = jnp.where(t == 0, front, back)
+
+    def send_rows(b):
+        with jax.named_scope("rows_pair"):
+            out_copy(b).wait_recv()
+        total = own_sum[b] + pair_in[b].astype(f32)
+        own_sum[b] = total
+
+        @pl.when(z != b)
+        def _():
+            row_out[b] = total.astype(bf16)
+            row_copy(b, z).start()
+
+
+    for u in range(UNITS):
+        spread(0, u)
+    own_tok.wait()
+    norm_block(z)
+    for u in range(3):
+        relay(0, u)
+    line_relay(tok_part, 0, 1)
+    send((QUERY,), True)
+    for u in range(3, UNITS):
+        relay(0, u)
+    line_relay(tok_part, 0, 2)
+    send((KEY, VALUE), True)
+    for d in others:
+        spread(d, LAT)
+    for d in others:
+        relay(d, LAT)
+    line_pair(tok_part, 0)
+    for d in others:
+        spread(d, QUERY)
+    pair_arrive(tok_part, 0, False)
+    for d in others:
+        norm_block(owner(d))
+    for d in range(n_sp):
+        arrive(d, LAT)
+
+    @pl.when(has(LAT, z))
+    def _():
+        multiply(LAT)
+        finish_lat()
+
+    for i in range(LAT_PARTS):
+        line_start(lat_part(i), i + 1)
+    for i in range(LAT_PARTS):
+        pair_own(lat_part(i), i + 1)
+    send((OUT_RET, OUT_ATT), False)
+    for d in others:
+        relay(d, QUERY)
+    for d in others:
+        spread(d, KEY)
+    project(QUERY)
+    for d in others:
+        relay(d, KEY)
+    for d in others:
+        spread(d, VALUE)
+    project(KEY)
+    for d in others:
+        relay(d, VALUE)
+    for distance in range(1, n_sp - 1):
+        for i in range(LAT_PARTS):
+            line_relay(lat_part(i), i + 1, distance)
+    send((OUT_RET, OUT_ATT), True)
+    project(VALUE)
+    for d in others:
+        shift_copy(d).wait_recv()
+    own_shift.wait()
+    own_state.wait()
+    own_kvup.wait()
+    own_qup.wait()
+    for b in range(n_sp):
+        with jax.named_scope(f"retention#b={b}"):
+            retention(b)
+    for i in range(LAT_PARTS):
+        line_pair(lat_part(i), i + 1)
+    for i in range(LAT_PARTS):
+        pair_arrive(lat_part(i), i + 1, True)
+    for i in range(n_sp):
+        with jax.named_scope(f"expand#b={i}"):
+            expand(i)
+    for d in others:
+        spread(d, OUT_RET)
+    for b in range(n_sp // 2):
+        attend(b)
+    for d in others:
+        relay(d, OUT_RET)
+    for b in range(n_sp // 2, n_sp):
+        attend(b)
+    for d in others:
+        spread(d, OUT_ATT)
+    for d in others:
+        relay(d, OUT_ATT)
+    for u in (OUT_RET, OUT_ATT):
+        for d in range(n_sp):
+            arrive(d, u)
+    upper = z // (n_sp // 2)
+    order = (3 - 3 * upper, 2 - upper, z + 1 - 2 * (z % 2), z)
+    for step, b in enumerate(order):
+        with jax.named_scope(f"out#b={step}"):
+            project_out(b)
         if step:
             send_rows(order[step - 1])
     send_rows(order[-1])
     total = own_sum[z]
-    for d in range(1, n_sp):
-        row_copy(0, owner(d)).wait_recv()
+    for d in others:
+        with jax.named_scope(f"rows#d={d}"):
+            row_copy(0, owner(d)).wait_recv()
         total = total + row_in[owner(d)].astype(f32)
     out_ref[...] = total.astype(bf16)
 
-    for group in (z_copies, x_copies, y_copies, f_copies, pair_copies):
-        for copy in group.values():
-            copy.wait_send()
+    for u in range(UNITS):
+        for d in range(n_sp):
+
+            def drain(d=d, u=u):
+                x_copy(d, u).wait_send()
+                y_copy(d, u).wait_send()
+                f_copy(d, u).wait_send()
+
+            when(has(u, z), drain)
+            if d:
+                to = (z + d) % n_sp
+                when(has(u, to), lambda d=d, u=u: z_copy(d, u).wait_send())
+    for d in others:
+        shift_copy(d).wait_send()
     line_drain(tok_part, 0, False)
-    for i in range(n_sp):
+    for i in range(LAT_PARTS):
         line_drain(lat_part(i), i + 1, True)
     for b in range(n_sp):
+        out_copy(b).wait_send()
         pl.when(z != b)(lambda b=b: row_copy(b, z).wait_send())
 
 
@@ -895,7 +1010,7 @@
             vmem((n_sp * 4 * w_rows, 6 * WIDE), bf16),
             vmem((n_sp,) + decay_shift.shape[1:], f32),
             vmem((length, width), bf16),
-            vmem((length, 4 * WIDE), f32),
+            vmem((length, WIDE), f32),
             vmem((length, WIDE), bf16),
             vmem((length, WIDE), bf16),
             vmem((length, WIDE), bf16),
@@ -914,21 +1029,9 @@
             vmem((n_sp, half, out_wide), bf16),
             vmem((n_sp, half, out_wide), bf16),
             dma((11,)),
-            dma((n_sp, 6)),
-            dma((n_sp, 6)),
-            dma((n_sp, 4)),
-            dma((n_sp, 4)),
-            dma((n_sp, 4)),
-            dma((n_sp, 4)),
-            dma((n_sp, 4)),
-            dma((n_sp, 4)),
-            dma((7, n_sp)),
-            dma((7, n_sp)),
-            dma((n_sp + 1, n_sp)),
-            dma((n_sp + 1, n_sp)),
-            dma((n_sp + 1, n_sp)),
-            dma((n_sp + 1, n_sp)),
-            dma((n_sp + 1, n_sp)),
+            *[dma((n_sp, UNITS))] * 8,
+            *[dma((3, n_sp))] * 2,
+            *[dma((LAT_PARTS + 1, n_sp))] * 5,
         ],
         compiler_params=pltpu.CompilerParams(
             collective_id=0, has_side_effects=True, vmem_limit_bytes=62 * 1024 * 1024

time: 134 us -> 116 us (0.87)
  Pallas kernels: 127 us -> 110 us
    pallas_call x1, Pallas kernels: 127 us -> 110 us  [heads_plan(): pl.pallas_call(functools.partial(layer_kernel, n_sp, q_wide, kv_wide), ou...]
where the time goes in v1:
time: 116 us; the launch traced here: 115 us
  Pallas kernels  110 us (95%)
  local copies, waits for them, and re-layouts  5.58 us (5%)
    pallas_call x1, Pallas kernels, heads_plan(): pl.pallas_call(functools.partial(layer_kernel, n_sp, q_wide, kv_wide), ou...  110 us
    unnamed x2, local copies, waits for them, and re-layouts  2.49 us

profile of v1, /device:TPU:9, one launch (start us, length us, event | category | flops | bytes accessed | tf_op | source)
XLA Modules:
  0.0 115.5 jit_solution(13922778193535234001)
XLA Ops:
  0.0 1.3 %broadcast_in_dim.17.qgain_ref = f32[1,768]{1,0:T(1,128)} reshape(f32[768]{0:T(1024)} %param.33) | data formatting | bytes 6144 | tf_op jit(solution)/shard_map/broadcast_in_dim | solution.py:1050
  1.3 0.8 copy.26
  2.1 0.1 fusion
  2.2 1.0 concatenate.3
  3.2 0.7 pad.4.lat_ref
  3.9 109.9 %shard_map.217 = bf16[64,2048]{1,0:T(8,128)(2,1)} custom-call(bf16[128,2048]{1,0:T(8,128)(2,1)} %bitcast.11, bf16[128,1024]{1,0:T(8,128)(2,1)} %pad.4.lat_ref, bf16[128,1024]{1,0:T(8,128)(2,1)} %wq_ref.1, bf16[128,1024]{1,0:T(8,128)(2,1)} %wk_ref.1, bf16[128,1024]{1,0:T(8,128)(2,1)} %wv_ref.1, bf16[128,1024]{1,0:T(8,128)(2,1)} %wr_ref.1, ...), custom_call_target="tpu_custom_call" | custom-call | tf_op jit(solution)/shard_map/pallas_call | solution.py:1003
  113.8 1.7 %copy.28 = bf16[1,64,2048]{2,1,0:T(8,128)(2,1)} copy(bf16[1,64,2048]{2,1,0:T(8,128)(2,1)} %bitcast.10) | data formatting | bytes 524288

commit v2 on v1

--- a/solution.py
+++ b/solution.py
@@ -300,7 +300,7 @@
         and up_wide == 2 * (NOPE_DIM + ROPE_DIM) * ret_local
         and q_wide % 128 == 0
         and kv_wide % 128 == 0
-        and q_wide + kv_wide + 2 * ROPE_DIM <= ret_local * WIDE
+        and q_wide == kv_wide + 2 * ROPE_DIM
     )
 
 
@@ -325,12 +325,14 @@
     q_wide,
     kv_wide,
     tok_ref,
-    lat_ref,
+    wqd_ref,
+    wkvd_ref,
     wq_ref,
     wk_ref,
     wv_ref,
     wr_ref,
     wa_ref,
+    rope_ref,
     shift_ref,
     rate_ref,
     gain_ref,
@@ -348,9 +350,12 @@
     out_ref,
     tok_all,
     w_all,
+    w_lat,
+    kv_src,
     shift_all,
     normed,
-    acc,
+    acc_ret,
+    acc_lat,
     ret_q,
     ret_k,
     ret_v,
@@ -393,9 +398,9 @@
     rows = tok_ref.shape[0]
     length = n_sp * rows
     half = rows // 2
-    weights = (lat_ref, wq_ref, wk_ref, wv_ref, wr_ref, wa_ref)
+    weights = (None, wq_ref, wk_ref, wv_ref, wr_ref, wa_ref)
     f32, bf16 = jnp.float32, jnp.bfloat16
-    lat_used = -(-(q_wide + kv_wide + 2 * ROPE_DIM) // WIDE)
+    q_place, kv_place = n_sp // 2 - 1, n_sp // 2
     others = range(1, n_sp)
 
     def remote(src, dst, send, recv, **where):
@@ -422,18 +427,26 @@
             return slice(i * size, (i + 1) * size)
         return pl.ds(pl.multiple_of(i * size, size), size)
 
-    def owner(d):
-        return (z + n_sp - d) % n_sp
+    upper = z // (n_sp // 2)
+    is_end = (z == 0) | (z == n_sp - 1)
+
+    def origin_of(k):
+        depth_in = z + upper * (n_sp - 1 - 2 * z)
+        found = (depth_in * 0, 1 + depth_in, 2 - 2 * depth_in, depth_in * 0 + 3)[k]
+        return z if k == 0 else found + upper * (n_sp - 1 - 2 * found)
 
 
     def piece(u, dest):
         return weights[u].at[:, at(dest, WIDE)]
 
     def part(owner_z, owner_f, u):
-        return w_all.at[at(owner_z * fs + owner_f), u * WIDE : (u + 1) * WIDE]
+        where = at(owner_z * fs + owner_f)
+        if u == LAT:
+            return w_lat.at[where]
+        return w_all.at[where, (u - 1) * WIDE : u * WIDE]
 
     def has(u, place):
-        return place < lat_used if u == LAT else True
+        return (place == q_place) | (place == kv_place) if u == LAT else True
 
     def when(condition, action):
         if condition is True:
@@ -441,45 +454,56 @@
         else:
             pl.when(condition)(action)
 
-    def z_copy(d, u):
-        to = (z + d) % n_sp
-        return remote(piece(u, to), part(z, f, u), z_send.at[d, u], z_recv.at[d, u], sp=to)
-
-    def x_copy(d, u):
-        ref = part(owner(d), f, u)
-        return remote(ref, ref, x_send.at[d, u], x_recv.at[d, u], fs=xn)
-
-    def y_copy(d, u):
-        ref = part(owner(d), f, u)
-        return remote(ref, ref, y_send.at[d, u], y_recv.at[d, u], fs=yn)
-
-    def f_copy(d, u):
-        source, to = (xn, yn) if (d + u) % 2 == 0 else (yn, xn)
-        ref = part(owner(d), source, u)
-        return remote(ref, ref, f_send.at[d, u], f_recv.at[d, u], fs=to)
+    lat_sources = {q_place: wqd_ref, kv_place: kv_src}
+
+    def z_copy(to, u, src=None):
+        return remote(
+            piece(u, to) if src is None else src,
+            part(z, f, u),
+            z_send.at[to, u],
+            z_recv.at[z, u],
+            sp=to,
+        )
+
+    def z_arrival(k, u):
+        ref = part(origin_of(k), f, u)
+        return remote(ref, ref, z_send.at[z, u], z_recv.at[origin_of(k), u], tp=other)
+
+    def x_copy(k, u):
+        ref = part(origin_of(k), f, u)
+        return remote(ref, ref, x_send.at[k, u], x_recv.at[k, u], fs=xn)
+
+    def y_copy(k, u):
+        ref = part(origin_of(k), f, u)
+        return remote(ref, ref, y_send.at[k, u], y_recv.at[k, u], fs=yn)
+
+    def f_copy(k, u):
+        source, to = (xn, yn) if (k + u) % 2 == 0 else (yn, xn)
+        ref = part(origin_of(k), source, u)
+        return remote(ref, ref, f_send.at[k, u], f_recv.at[k, u], fs=to)
 
     def own_copy(u):
         return pltpu.make_async_copy(piece(u, z), part(z, f, u), local_sem.at[u])
 
-    def on_relay_link(to):
-        return ((z == 1) & (to == 0)) | ((z == n_sp - 2) & (to == n_sp - 1))
-
-    def send(units, held):
-        for u in units:
-            for d in others:
-                to = (z + d) % n_sp
-                condition = on_relay_link(to) if held else ~on_relay_link(to)
-                if u == LAT:
-                    condition = condition & has(u, to)
-                pl.when(condition)(lambda d=d, u=u: z_copy(d, u).start())
+    def own_lat_copy(place):
+        return pltpu.make_async_copy(lat_sources[place], part(z, f, LAT), local_sem.at[LAT])
+
+    def send(u):
+        for k in others:
+            z_copy(origin_of(k), u).start()
+
+    def send_lat(place):
+        pl.when(z != place)(lambda: z_copy(place, LAT, lat_sources[place]).start())
 
     def spread(d, u):
         def action():
             with jax.named_scope(f"spread#d={d}#u={u}"):
-                if d == 0:
+                if d:
+                    z_arrival(d, u).wait_recv()
+                elif u == LAT:
+                    own_lat_copy(q_place).wait()
+                else:
                     own_copy(u).wait()
-                else:
-                    z_copy(d, u).wait_recv()
             x_copy(d, u).start()
             y_copy(d, u).start()
 
@@ -510,13 +534,16 @@
     lat_rows = length // LAT_PARTS
 
     def lat_part(i):
-        return lambda origin: lat_all.at[t, origin, pl.ds(i * lat_rows, lat_rows)]
+        return lambda origin: lat_all.at[t, origin - q_place, pl.ds(i * lat_rows, lat_rows)]
 
     def sends(row, origin):
-        return True if row == 0 else origin < lat_used
+        return True if row == 0 else has(LAT, origin)
 
     def both(condition, more):
         return condition if more is True else condition & more
+
+    def steps(row):
+        return range(1, n_sp - 1 if row == 0 else 2)
 
     def line_copy(where, row, dest, src=None):
         return remote(
@@ -539,8 +566,8 @@
         near = (z - dest == 1) | (dest - z == 1)
         return near if dest in (0, n_sp - 1) else z != dest
 
-    def line_start(where, row, src=None):
-        for distance in others:
+    def line_start(where, row, src=None, distances=others):
+        for distance in distances:
             for dest in range(n_sp):
                 condition = direct(dest) & ((z - dest == distance) | (dest - z == distance))
                 pl.when(both(condition, sends(row, z)))(
@@ -593,7 +620,7 @@
                 lambda dest=dest: line_copy(where, row, dest).wait_send()
             )
         for middle, dest in ends:
-            for distance in range(1, n_sp - 1):
+            for distance in steps(row):
                 origin = middle + (middle - dest) * distance
                 pl.when(both(z == middle, sends(row, origin)))(
                     lambda origin=origin, dest=dest: relay_copy(
@@ -609,25 +636,23 @@
         return remote(shift_ref, shift_all.at[z], m_send.at[0, d], m_recv.at[0, d], sp=to)
 
 
-    line_start(tok_part, 0, tok_ref.at[mine])
-    for d in others:
-        shift_copy(d).start()
-    for u in range(UNITS):
-        when(has(u, z), lambda u=u: own_copy(u).start())
-    send((LAT,), True)
-    send((LAT, QUERY, KEY, VALUE), False)
+    def start_inputs():
+        own_tok.start()
+        own_shift.start()
+        own_kvup.start()
+        own_qup.start()
+        own_state.start()
+        for d in others:
+            shift_copy(d).start()
+
     own_tok = pltpu.make_async_copy(tok_ref, tok_all.at[z], local_sem.at[6])
-    own_tok.start()
     own_shift = pltpu.make_async_copy(shift_ref, shift_all.at[z], local_sem.at[7])
-    own_shift.start()
     att_wide = kvup.shape[1]
     own_kvup = pltpu.make_async_copy(kvup_ref.at[:, at(z, att_wide)], kvup, local_sem.at[8])
-    own_kvup.start()
+    own_state = pltpu.make_async_copy(start_ref.at[z], state, local_sem.at[9])
     up_wide = qup.shape[1]
     own_qup = pltpu.make_async_copy(qup_ref.at[:, at(z, up_wide)], qup, local_sem.at[10])
-    own_qup.start()
-    own_state = pltpu.make_async_copy(start_ref.at[z], state, local_sem.at[9])
-    own_state.start()
+    own_kvd = pltpu.make_async_copy(wkvd_ref, kv_src.at[:, :kv_wide], local_sem.at[11])
 
     def norm_block(i):
         x = tok_all[i].astype(f32)
@@ -637,10 +662,14 @@
     depth = fs * rows
 
     def multiply(u):
+        weight, columns = (
+            (w_lat, slice(None)) if u == LAT else (w_all, slice((u - 1) * WIDE, u * WIDE))
+        )
+        acc = acc_lat if u == LAT else acc_ret
         with jax.named_scope(f"multiply#u={u}"):
             acc[...] = jnp.dot(
                 normed[:, :depth],
-                w_all[:depth, u * WIDE : (u + 1) * WIDE],
+                weight[:depth, columns],
                 preferred_element_type=f32,
             )
 
@@ -648,29 +677,25 @@
                 begin = at(i, depth)
                 acc[...] += jnp.dot(
                     normed[:, begin],
-                    w_all[begin, u * WIDE : (u + 1) * WIDE],
+                    weight[begin, columns],
                     preferred_element_type=f32,
                 )
                 return carry
 
             lax.fori_loop(1, n_sp, chunk, 0)
 
-    rope_index = (q_wide + kv_wide) // WIDE
-    rope_lane = (q_wide + kv_wide) % WIDE
     rd = RET_DIM // 2
 
     def finish_lat():
         def block(i, carry):
-            raw = acc[at(i), :]
-            pair = raw[:, rope_lane : rope_lane + 2 * ROPE_DIM]
+            lat_all[t, z - q_place, at(i), :kv_wide] = acc_lat[at(i), :kv_wide].astype(bf16)
+            pair = acc_lat[at(i), kv_wide:]
             turned = pair * pcos_ref[at(i), :] + pltpu.roll(pair, ROPE_DIM, 1) * psin_ref[at(i), :]
             lane = lax.broadcasted_iota(jnp.int32, turned.shape, 1)
             turned = jnp.where(lane < ROPE_DIM, turned, pltpu.roll(turned, ROPE_DIM, 1))
-            pieces = [raw[:, :rope_lane]] if rope_lane else []
-            pieces.append(jnp.where(z == rope_index, turned, pair))
-            if rope_lane + 2 * ROPE_DIM < WIDE:
-                pieces.append(raw[:, rope_lane + 2 * ROPE_DIM :])
-            lat_all[t, z, at(i), :] = jnp.concatenate(pieces, axis=1).astype(bf16)
+            lat_all[t, z - q_place, at(i), kv_wide:] = jnp.where(
+                z == kv_place, turned, pair
+            ).astype(bf16)
             return carry
 
         lax.fori_loop(0, n_sp, block, 0)
@@ -678,7 +703,7 @@
     def finish_turned(dst, factor):
         def block(i, carry):
             cosine, sine = rcos_ref[at(i), :], rsin_ref[at(i), :]
-            a, b = acc[at(i), :rd], acc[at(i), rd:]
+            a, b = acc_ret[at(i), :rd], acc_ret[at(i), rd:]
             dst[at(i), :rd] = ((a * cosine - b * sine) * factor).astype(bf16)
             dst[at(i), rd:] = ((b * cosine + a * sine) * factor).astype(bf16)
             return carry
@@ -694,7 +719,7 @@
         elif u == KEY:
             finish_turned(ret_k, RET_DIM ** (-0.5))
         else:
-            ret_v[...] = acc[...].astype(bf16)
+            ret_v[...] = acc_ret[...].astype(bf16)
 
     r_iota = lax.broadcasted_iota(jnp.int32, (rows, rows), 0)
     c_iota = lax.broadcasted_iota(jnp.int32, (rows, rows), 1)
@@ -731,27 +756,17 @@
             bf16
         )
 
-    def chunks(first, count):
-        found = []
-        for core in range(2):
-            for j in range(count // 128):
-                lane = first + j * 128
-                found.append((core, lane // WIDE, lane % WIDE))
-        return found
-
-    q_chunks, kv_chunks = chunks(0, q_wide), chunks(q_wide, kv_wide)
-    rope_at = (rope_index, rope_lane)
     att_heads = att_wide // (NOPE_DIM + VAL_DIM)
 
     def expand(i):
-        def latent(found, gain):
+        def latent(slot, wide, gain):
             x = jnp.concatenate(
-                [lat_all[c, s, at(i), lane : lane + 128] for c, s, lane in found], axis=1
+                [lat_all[core, slot, at(i), :wide] for core in range(2)], axis=1
             ).astype(f32)
             scaled = x * lax.rsqrt(jnp.mean(x * x, axis=-1, keepdims=True) + EPSILON)
             return (scaled * gain[...]).astype(bf16)
 
-        query = jnp.dot(latent(q_chunks, qgain_ref), qup[...], preferred_element_type=f32)
+        query = jnp.dot(latent(0, q_wide, qgain_ref), qup[...], preferred_element_type=f32)
         first, middle, end = query[:, :128], query[:, 128:256], query[:, 256:]
         lane = lax.broadcasted_iota(jnp.int32, first.shape, 1)
         second = jnp.where(
@@ -768,9 +783,9 @@
         qn[at(i), NOPE_DIM:] = second.astype(bf16)
         qr[at(i), :] = (pair * pcos_ref[at(i), :] + swapped * psin_ref[at(i), :]).astype(bf16)
         expanded[at(i), :] = jnp.dot(
-            latent(kv_chunks, kvgain_ref), kvup[...], preferred_element_type=f32
+            latent(1, kv_wide, kvgain_ref), kvup[...], preferred_element_type=f32
         ).astype(bf16)
-        rope_key[at(i), :] = lat_all[0, rope_at[0], at(i), rope_at[1] : rope_at[1] + 128]
+        rope_key[at(i), :] = lat_all[0, 1, at(i), kv_wide:]
 
     scale = (NOPE_DIM + ROPE_DIM) ** (-0.5)
 
@@ -814,7 +829,7 @@
     def project_out(b):
         got = lax.dot_general(
             merged[at(b), :],
-            w_all[:, OUT_RET * WIDE :],
+            w_all[:, (OUT_RET - 1) * WIDE :],
             CONTRACT,
             preferred_element_type=f32,
         )
@@ -835,57 +850,138 @@
             row_copy(b, z).start()
 
 
-    for u in range(UNITS):
-        spread(0, u)
-    own_tok.wait()
-    norm_block(z)
-    for u in range(3):
-        relay(0, u)
-    line_relay(tok_part, 0, 1)
-    send((QUERY,), True)
-    for u in range(3, UNITS):
-        relay(0, u)
-    line_relay(tok_part, 0, 2)
-    send((KEY, VALUE), True)
-    for d in others:
-        spread(d, LAT)
-    for d in others:
-        relay(d, LAT)
-    line_pair(tok_part, 0)
-    for d in others:
-        spread(d, QUERY)
-    pair_arrive(tok_part, 0, False)
-    for d in others:
-        norm_block(owner(d))
-    for d in range(n_sp):
-        arrive(d, LAT)
-
-    @pl.when(has(LAT, z))
+    def many(action, *pairs):
+        for k, u in pairs:
+            action(k, u)
+
+    def norm_others():
+        pair_arrive(tok_part, 0, False)
+        for k in others:
+            norm_block(origin_of(k))
+
+    def send_near_end(u):
+        for dest in (0, n_sp - 1):
+            pl.when(direct(dest))(lambda dest=dest: z_copy(dest, u).start())
+
+    def send_far_end(u):
+        for dest in (0, n_sp - 1):
+            pl.when((z - dest == 2) | (dest - z == 2))(lambda dest=dest: z_copy(dest, u).start())
+
+    def send_middle(u):
+        for dest in lat_sources:
+            pl.when(z != dest)(lambda dest=dest: z_copy(dest, u).start())
+
+    ret_weights = (QUERY, KEY, VALUE)
+    out_weights = (OUT_RET, OUT_ATT)
+
+    own_kvd.start()
+    pl.when(~is_end)(lambda: line_start(tok_part, 0, tok_ref.at[mine]))
+
+    @pl.when(z == q_place)
     def _():
+        own_lat_copy(q_place).start()
+
+    for u in ret_weights + out_weights:
+        own_copy(u).start()
+    send_lat(q_place)
+    for u in ret_weights + out_weights:
+        send_near_end(u)
+    with jax.named_scope("kvsrc"):
+        own_kvd.wait()
+    rope = rope_ref[...]
+    kv_src[:, kv_wide:] = jnp.concatenate(
+        [rope, rope[:, ROPE_DIM // 2 :], rope[:, : ROPE_DIM // 2]], axis=1
+    )
+
+    @pl.when(z == kv_place)
+    def _():
+        own_lat_copy(kv_place).start()
+
+    send_lat(kv_place)
+
+    @pl.when(is_end)
+    def _():
+        line_start(tok_part, 0, tok_ref.at[mine], (2, 1))
+        for u in ret_weights:
+            send(u)
+        start_inputs()
+        many(spread, (0, QUERY), (0, KEY), (0, VALUE), (0, OUT_RET), (0, OUT_ATT))
+        own_tok.wait()
+        norm_block(z)
+        many(spread, (1, QUERY), (1, KEY))
+        many(relay, (0, QUERY), (0, KEY))
+        many(spread, (1, VALUE))
+        many(relay, (0, VALUE))
+        many(spread, (1, OUT_RET), (1, OUT_ATT))
+        many(relay, (0, OUT_RET), (0, OUT_ATT))
+        many(relay, (1, QUERY), (1, KEY))
+        many(spread, (2, QUERY))
+        many(relay, (1, VALUE))
+        many(spread, (2, KEY))
+        many(relay, (1, OUT_RET), (1, OUT_ATT))
+        many(spread, (2, VALUE))
+        many(relay, (2, QUERY), (2, KEY))
+        many(spread, (3, QUERY))
+        many(relay, (2, VALUE))
+        many(spread, (3, KEY))
+        many(relay, (3, QUERY))
+        many(spread, (3, VALUE))
+        many(relay, (3, KEY))
+        line_pair(tok_part, 0)
+        send(OUT_RET)
+        send(OUT_ATT)
+        norm_others()
+        project(QUERY)
+        many(relay, (3, VALUE))
+        project(KEY)
+
+    @pl.when(~is_end)
+    def _():
+        for u in ret_weights:
+            send_far_end(u)
+        for u in ret_weights:
+            send_middle(u)
+        start_inputs()
+        many(spread, (0, LAT), (0, QUERY), (0, KEY))
+        many(relay, (0, LAT))
+        many(spread, (2, LAT), (3, LAT), (0, VALUE))
+        own_tok.wait()
+        norm_block(z)
+        many(relay, (0, QUERY), (0, KEY), (2, LAT))
+        line_relay(tok_part, 0, 1)
+        many(spread, (1, LAT), (0, OUT_RET), (0, OUT_ATT))
+        many(relay, (3, LAT), (0, VALUE), (1, LAT))
+        line_relay(tok_part, 0, 2)
+        line_pair(tok_part, 0)
+        many(relay, (0, OUT_RET), (0, OUT_ATT))
+        norm_others()
+        for k in range(n_sp):
+            arrive(k, LAT)
         multiply(LAT)
         finish_lat()
-
-    for i in range(LAT_PARTS):
-        line_start(lat_part(i), i + 1)
-    for i in range(LAT_PARTS):
-        pair_own(lat_part(i), i + 1)
-    send((OUT_RET, OUT_ATT), False)
-    for d in others:
-        relay(d, QUERY)
-    for d in others:
-        spread(d, KEY)
-    project(QUERY)
-    for d in others:
-        relay(d, KEY)
-    for d in others:
-        spread(d, VALUE)
-    project(KEY)
-    for d in others:
-        relay(d, VALUE)
-    for distance in range(1, n_sp - 1):
         for i in range(LAT_PARTS):
-            line_relay(lat_part(i), i + 1, distance)
-    send((OUT_RET, OUT_ATT), True)
+            line_start(lat_part(i), i + 1)
+        for i in range(LAT_PARTS):
+            pair_own(lat_part(i), i + 1)
+        for u in out_weights:
+            send_middle(u)
+            send_far_end(u)
+        many(spread, (1, QUERY), (2, QUERY), (3, QUERY))
+        many(spread, (1, KEY), (2, KEY))
+        many(relay, (1, QUERY), (2, QUERY), (3, QUERY))
+        many(spread, (3, KEY), (1, VALUE), (2, VALUE))
+        many(relay, (1, KEY), (2, KEY))
+        many(spread, (3, VALUE))
+        line_relay(lat_part(0), 1, 1)
+        many(relay, (3, KEY))
+        project(QUERY)
+        many(relay, (1, VALUE), (2, VALUE))
+        many(spread, (1, OUT_RET))
+        line_relay(lat_part(1), 2, 1)
+        many(relay, (3, VALUE))
+        project(KEY)
+        many(spread, (1, OUT_ATT))
+
     project(VALUE)
     for d in others:
         shift_copy(d).wait_recv()
@@ -893,32 +989,33 @@
     own_state.wait()
     own_kvup.wait()
     own_qup.wait()
+    many(spread, (2, OUT_RET))
     for b in range(n_sp):
         with jax.named_scope(f"retention#b={b}"):
             retention(b)
+    many(spread, (3, OUT_RET), (2, OUT_ATT))
+    pl.when(~is_end)(lambda: many(relay, (1, OUT_RET)))
+    many(relay, (2, OUT_RET))
+    many(spread, (3, OUT_ATT))
+    pl.when(~is_end)(lambda: many(relay, (1, OUT_ATT)))
+
+    blocks = n_sp // LAT_PARTS
     for i in range(LAT_PARTS):
         line_pair(lat_part(i), i + 1)
-    for i in range(LAT_PARTS):
+        if i == 0:
+            many(relay, (3, OUT_RET))
+        else:
+            many(relay, (2, OUT_ATT), (3, OUT_ATT))
         pair_arrive(lat_part(i), i + 1, True)
-    for i in range(n_sp):
-        with jax.named_scope(f"expand#b={i}"):
-            expand(i)
-    for d in others:
-        spread(d, OUT_RET)
-    for b in range(n_sp // 2):
-        attend(b)
-    for d in others:
-        relay(d, OUT_RET)
-    for b in range(n_sp // 2, n_sp):
-        attend(b)
-    for d in others:
-        spread(d, OUT_ATT)
-    for d in others:
-        relay(d, OUT_ATT)
-    for u in (OUT_RET, OUT_ATT):
-        for d in range(n_sp):
-            arrive(d, u)
-    upper = z // (n_sp // 2)
+        for b in range(i * blocks, (i + 1) * blocks):
+            with jax.named_scope(f"expand#b={b}"):
+                expand(b)
+        for b in range(i * blocks, (i + 1) * blocks):
+            with jax.named_scope(f"attend#b={b}"):
+                attend(b)
+    for u in out_weights:
+        for k in range(n_sp):
+            arrive(k, u)
     order = (3 - 3 * upper, 2 - upper, z + 1 - 2 * (z % 2), z)
     for step, b in enumerate(order):
         with jax.named_scope(f"out#b={step}"):
@@ -927,24 +1024,27 @@
             send_rows(order[step - 1])
     send_rows(order[-1])
     total = own_sum[z]
-    for d in others:
-        with jax.named_scope(f"rows#d={d}"):
-            row_copy(0, owner(d)).wait_recv()
-        total = total + row_in[owner(d)].astype(f32)
+    for k in others:
+        with jax.named_scope(f"rows#k={k}"):
+            row_copy(0, origin_of(k)).wait_recv()
+        total = total + row_in[origin_of(k)].astype(f32)
     out_ref[...] = total.astype(bf16)
 
     for u in range(UNITS):
-        for d in range(n_sp):
-
-            def drain(d=d, u=u):
-                x_copy(d, u).wait_send()
-                y_copy(d, u).wait_send()
-                f_copy(d, u).wait_send()
+        for k in range(n_sp):
+
+            def drain(k=k, u=u):
+                x_copy(k, u).wait_send()
+                y_copy(k, u).wait_send()
+                f_copy(k, u).wait_send()
 
             when(has(u, z), drain)
-            if d:
-                to = (z + d) % n_sp
-                when(has(u, to), lambda d=d, u=u: z_copy(d, u).wait_send())
+            if k and u != LAT:
+                z_copy(origin_of(k), u).wait_send()
+    for place in lat_sources:
+        pl.when(z != place)(
+            lambda place=place: z_copy(place, LAT, lat_sources[place]).wait_send()
+        )
     for d in others:
         shift_copy(d).wait_send()
     line_drain(tok_part, 0, False)
@@ -980,15 +1080,9 @@
     rows, width = tokens.shape[1:]
     length = n_sp * rows
     q_wide, kv_wide = w_q_down.shape[1], w_kv_down.shape[1]
-    rope_half = ROPE_DIM // 2
     w_rows = w_q_down.shape[0]
     att_heads = w_q_up.shape[1] // (NOPE_DIM + ROPE_DIM) // n_sp
 
-    def swap(x):
-        return jnp.concatenate([x[..., rope_half:], x[..., :rope_half]], axis=-1)
-
-    lat = jnp.concatenate([w_q_down, w_kv_down, w_rope_key, swap(w_rope_key)], axis=1)
-    lat = jnp.pad(lat, ((0, 0), (0, n_sp * WIDE - lat.shape[1])))
     ret_cos, ret_sin = wave_tables(length, RET_DIM)
     rope_cos, rope_sin = wave_tables(length, ROPE_DIM)
     pair_cos = np.concatenate([rope_cos] * 4, axis=1)
@@ -1003,18 +1097,21 @@
     mixed = pl.pallas_call(
         functools.partial(layer_kernel, n_sp, q_wide, kv_wide),
         out_shape=jax.ShapeDtypeStruct((half, out_wide), bf16),
-        in_specs=[any_spec] * 8 + [vmem_spec] * 10 + [any_spec] * 3,
+        in_specs=[any_spec] * 8 + [vmem_spec, any_spec] + [vmem_spec] * 10 + [any_spec] * 3,
         out_specs=vmem_spec,
         scratch_shapes=[
             vmem((n_sp, rows, width), bf16),
-            vmem((n_sp * 4 * w_rows, 6 * WIDE), bf16),
+            vmem((n_sp * 4 * w_rows, (UNITS - 1) * WIDE), bf16),
+            vmem((n_sp * 4 * w_rows, q_wide), bf16),
+            vmem((w_rows, q_wide), bf16),
             vmem((n_sp,) + decay_shift.shape[1:], f32),
             vmem((length, width), bf16),
             vmem((length, WIDE), f32),
+            vmem((length, q_wide), f32),
             vmem((length, WIDE), bf16),
             vmem((length, WIDE), bf16),
             vmem((length, WIDE), bf16),
-            vmem((2, n_sp, length, WIDE), bf16),
+            vmem((2, 2, length, q_wide), bf16),
             vmem((RET_DIM, RET_DIM), f32),
             vmem((length, att_heads * NOPE_DIM), bf16),
             vmem((length, att_heads * ROPE_DIM), bf16),
@@ -1028,7 +1125,7 @@
             vmem((n_sp, half, out_wide), bf16),
             vmem((n_sp, half, out_wide), bf16),
             vmem((n_sp, half, out_wide), bf16),
-            dma((11,)),
+            dma((12,)),
             *[dma((n_sp, UNITS))] * 8,
             *[dma((3, n_sp))] * 2,
             *[dma((LAT_PARTS + 1, n_sp))] * 5,
@@ -1038,12 +1135,14 @@
         ),
     )(
         tokens[0],
-        lat,
+        w_q_down,
+        w_kv_down,
         w_ret_query,
         w_ret_key,
         w_ret_value,
         w_ret_out,
         w_att_out,
+        w_rope_key,
         decay_shift[0],
         head_rate[None],
         norm_gain[None],

time: 116 us -> 104 us (0.90)
  Pallas kernels: 110 us -> 99.4 us
  local copies, waits for them, and re-layouts: 5.58 us -> 4.37 us
    pallas_call x1, Pallas kernels: 110 us -> 99.4 us  [heads_plan(): pl.pallas_call(functools.partial(layer_kernel, n_sp, q_wide, kv_wide), ou...]
where the time goes in v2:
time: 104 us
  Pallas kernels  99.4 us (96%)
  local copies, waits for them, and re-layouts  4.37 us (4%)
    pallas_call x1, Pallas kernels, heads_plan(): pl.pallas_call(functools.partial(layer_kernel, n_sp, q_wide, kv_wide), ou...  99.4 us
    unnamed x2, local copies, waits for them, and re-layouts  3.1 us

profile of v2, /device:TPU:9, one launch (start us, length us, event | category | flops | bytes accessed | tf_op | source)
XLA Modules:
  0.0 103.8 jit_solution(16649608093871951538)
XLA Ops:
  0.0 1.3 %broadcast_in_dim.17.qgain_ref = f32[1,768]{1,0:T(1,128)} reshape(f32[768]{0:T(1024)} %param.33) | data formatting | bytes 6144 | tf_op jit(solution)/shard_map/broadcast_in_dim | solution.py:1149
  1.3 1.4 %copy.24.rope_ref = bf16[128,64]{1,0:T(8,128)(2,1)} copy(bf16[128,64]{0,1:T(8,128)(2,1)} %param.30) | data formatting | bytes 32768 | tf_op args[7]
  2.7 99.4 %shard_map.217 = bf16[64,2048]{1,0:T(8,128)(2,1)} custom-call(bf16[128,2048]{1,0:T(8,128)(2,1)} %bitcast.11, bf16[128,384]{1,0:T(8,128)(2,1)} %wqd_ref.1, bf16[128,256]{1,0:T(8,128)(2,1)} %wkvd_ref.1, bf16[128,1024]{1,0:T(8,128)(2,1)} %wq_ref.1, bf16[128,1024]{1,0:T(8,128)(2,1)} %wk_ref.1, bf16[128,1024]{1,0:T(8,128)(2,1)} %wv_ref.1, ...), custom_call_target="tpu_custom_call" | custom-call | tf_op jit(solution)/shard_map/pallas_call | solution.py:1097
  102.1 1.7 %copy.26 = bf16[1,64,2048]{2,1,0:T(8,128)(2,1)} copy(bf16[1,64,2048]{2,1,0:T(8,128)(2,1)} %bitcast.10) | data formatting | bytes 524288

commit v3 on v2

--- a/solution.py
+++ b/solution.py
@@ -287,6 +287,8 @@
 UNITS = 6
 LAT, QUERY, KEY, VALUE, OUT_RET, OUT_ATT = range(UNITS)
 LAT_PARTS = 2
+OUT_PARTS = 2
+LEAD = 5
 
 
 def heads_fit(mesh, ret_local, sequences, q_wide, kv_wide, up_wide):
@@ -332,8 +334,27 @@
     wv_ref,
     wr_ref,
     wa_ref,
-    rope_ref,
+    rope_hbm,
     shift_ref,
+    rate_hbm,
+    gain_hbm,
+    qgain_hbm,
+    kvgain_hbm,
+    again_hbm,
+    rgain_hbm,
+    rcos_hbm,
+    rsin_hbm,
+    pcos_hbm,
+    psin_hbm,
+    qup_ref,
+    kvup_ref,
+    start_ref,
+    out_ref,
+    tok_all,
+    w_all,
+    w_lat,
+    kv_src,
+    rope_vmem,
     rate_ref,
     gain_ref,
     qgain_ref,
@@ -344,14 +365,6 @@
     rsin_ref,
     pcos_ref,
     psin_ref,
-    qup_ref,
-    kvup_ref,
-    start_ref,
-    out_ref,
-    tok_all,
-    w_all,
-    w_lat,
-    kv_src,
     shift_all,
     normed,
     acc_ret,
@@ -373,6 +386,7 @@
     pair_in,
     row_out,
     row_in,
+    far_in,
     local_sem,
     z_send,
     z_recv,
@@ -384,6 +398,12 @@
     f_recv,
     m_send,
     m_recv,
+    small_sem,
+    o_send,
+    o_recv,
+    r_send,
+    r_recv,
+    far_recv,
     l_send,
     l_recv,
     l_relay,
@@ -636,7 +656,31 @@
         return remote(shift_ref, shift_all.at[z], m_send.at[0, d], m_recv.at[0, d], sp=to)
 
 
+    staged = (
+        (rope_hbm, rope_vmem),
+        (rate_hbm, rate_ref),
+        (gain_hbm, gain_ref),
+        (qgain_hbm, qgain_ref),
+        (kvgain_hbm, kvgain_ref),
+        (again_hbm, again_ref),
+        (rgain_hbm, rgain_ref),
+        (rcos_hbm, rcos_ref),
+        (rsin_hbm, rsin_ref),
+        (pcos_hbm, pcos_ref),
+        (psin_hbm, psin_ref),
+    )
+    staged_copies = [
+        pltpu.make_async_copy(src, dst, small_sem.at[i]) for i, (src, dst) in enumerate(staged)
+    ]
+    small_copies, table_copies = staged_copies[:7], staged_copies[7:]
+
+    def wait_tables():
+        for copy in table_copies:
+            copy.wait()
+
     def start_inputs():
+        for copy in table_copies:
+            copy.start()
         own_tok.start()
         own_shift.start()
         own_kvup.start()
@@ -764,7 +808,7 @@
                 [lat_all[core, slot, at(i), :wide] for core in range(2)], axis=1
             ).astype(f32)
             scaled = x * lax.rsqrt(jnp.mean(x * x, axis=-1, keepdims=True) + EPSILON)
-            return (scaled * gain[...]).astype(bf16)
+            return (scaled * gain[...].reshape(1, wide * 2)).astype(bf16)
 
         query = jnp.dot(latent(0, q_wide, qgain_ref), qup[...], preferred_element_type=f32)
         first, middle, end = query[:, :128], query[:, 128:256], query[:, 256:]
@@ -820,34 +864,80 @@
                 scaled * gain
             ).astype(bf16)
 
-    def out_copy(b):
-        return remote(pair_out.at[b], pair_in.at[b], m_send.at[1, b], m_recv.at[1, b], tp=other)
-
-    def row_copy(b, origin):
-        return remote(row_out.at[b], row_in.at[origin], m_send.at[2, b], m_recv.at[2, origin], sp=b)
-
-    def project_out(b):
+
+    part_wide = out_ref.shape[1] // OUT_PARTS
+
+    def out_place(j):
+        depth_in = z + upper * (n_sp - 1 - 2 * z)
+        found = (depth_in * 0 + 3, depth_in * 0 + 2, 1 - depth_in, depth_in)[j]
+        return found + upper * (n_sp - 1 - 2 * found)
+
+    def out_columns(c):
+        return slice(c * part_wide, (c + 1) * part_wide)
+
+    def pair_sum(j, c):
+        return remote(
+            pair_out.at[j, c], pair_in.at[j, c], o_send.at[j, c], o_recv.at[j, c], tp=other
+        )
+
+    def near_rows(j, c):
+        return remote(
+            row_out.at[j, c], row_in.at[0, c], r_send.at[j, c], r_recv.at[0, c], sp=out_place(j)
+        )
+
+    def far_rows(j, c):
+        return remote(
+            row_out.at[j, c],
+            far_in.at[j, c],
+            r_send.at[j, c],
+            far_recv.at[j, c],
+            sp=z + 1 - 2 * upper,
+        )
+
+    def sum_rows(j, c):
+        return remote(
+            row_out.at[j, c], row_in.at[1, c], r_send.at[j, c], r_recv.at[1, c], sp=out_place(j)
+        )
+
+    def rows_arrival(k, c):
+        return remote(row_in.at[k, c], row_in.at[k, c], r_send.at[0, c], r_recv.at[k, c], tp=other)
+
+    def project_out(j, c):
+        first = slice(c * part_wide, (c + 1) * part_wide)
         got = lax.dot_general(
-            merged[at(b), :],
-            w_all[:, (OUT_RET - 1) * WIDE :],
+            merged[at(out_place(j)), :],
+            w_all[first, (OUT_RET - 1) * WIDE :],
             CONTRACT,
             preferred_element_type=f32,
         )
         front, back = got[:half, :], got[half:, :]
-        pair_out[b] = jnp.where(t == 0, back, front).astype(bf16)
-        out_copy(b).start()
-        own_sum[b] = jnp.where(t == 0, front, back)
-
-    def send_rows(b):
+        pair_out[j, c] = jnp.where(t == 0, back, front).astype(bf16)
+        pair_sum(j, c).start()
+        own_sum[j, :, out_columns(c)] = jnp.where(t == 0, front, back)
+
+    def finish_out(j, c):
         with jax.named_scope("rows_pair"):
-            out_copy(b).wait_recv()
-        total = own_sum[b] + pair_in[b].astype(f32)
-        own_sum[b] = total
-
-        @pl.when(z != b)
-        def _():
-            row_out[b] = total.astype(bf16)
-            row_copy(b, z).start()
+            pair_sum(j, c).wait_recv()
+        total = own_sum[j, :, out_columns(c)] + pair_in[j, c].astype(f32)
+        own_sum[j, :, out_columns(c)] = total
+        if j == n_sp - 1:
+            return
+
+        def ship(copy):
+            row_out[j, c] = total.astype(bf16)
+            copy.start()
+
+        if j == n_sp - 2:
+            ship(near_rows(j, c))
+        else:
+            pl.when(is_end)(lambda: ship(far_rows(j, c)))
+
+    def combine(j, c):
+        with jax.named_scope("combine"):
+            far_rows(j, c).wait_recv()
+        total = own_sum[j, :, out_columns(c)] + far_in[j, c].astype(f32)
+        row_out[j, c] = total.astype(bf16)
+        sum_rows(j, c).start()
 
 
     def many(action, *pairs):
@@ -875,6 +965,8 @@
     out_weights = (OUT_RET, OUT_ATT)
 
     own_kvd.start()
+    for copy in small_copies:
+        copy.start()
     pl.when(~is_end)(lambda: line_start(tok_part, 0, tok_ref.at[mine]))
 
     @pl.when(z == q_place)
@@ -888,7 +980,9 @@
         send_near_end(u)
     with jax.named_scope("kvsrc"):
         own_kvd.wait()
-    rope = rope_ref[...]
+        for copy in small_copies:
+            copy.wait()
+    rope = rope_vmem[...].astype(f32).T.astype(bf16)
     kv_src[:, kv_wide:] = jnp.concatenate(
         [rope, rope[:, ROPE_DIM // 2 :], rope[:, : ROPE_DIM // 2]], axis=1
     )
@@ -904,6 +998,8 @@
         line_start(tok_part, 0, tok_ref.at[mine], (2, 1))
         for u in ret_weights:
             send(u)
+        for u in out_weights:
+            z_copy(origin_of(1), u).start()
         start_inputs()
         many(spread, (0, QUERY), (0, KEY), (0, VALUE), (0, OUT_RET), (0, OUT_ATT))
         own_tok.wait()
@@ -928,9 +1024,11 @@
         many(spread, (3, VALUE))
         many(relay, (3, KEY))
         line_pair(tok_part, 0)
-        send(OUT_RET)
-        send(OUT_ATT)
+        for u in out_weights:
+            z_copy(origin_of(2), u).start()
+            z_copy(origin_of(3), u).start()
         norm_others()
+        wait_tables()
         project(QUERY)
         many(relay, (3, VALUE))
         project(KEY)
@@ -951,12 +1049,16 @@
         line_relay(tok_part, 0, 1)
         many(spread, (1, LAT), (0, OUT_RET), (0, OUT_ATT))
         many(relay, (3, LAT), (0, VALUE), (1, LAT))
+        many(spread, (2, QUERY))
         line_relay(tok_part, 0, 2)
         line_pair(tok_part, 0)
         many(relay, (0, OUT_RET), (0, OUT_ATT))
+        many(spread, (3, QUERY), (2, KEY))
         norm_others()
+        many(relay, (2, QUERY))
         for k in range(n_sp):
             arrive(k, LAT)
+        wait_tables()
         multiply(LAT)
         finish_lat()
         for i in range(LAT_PARTS):
@@ -966,21 +1068,24 @@
         for u in out_weights:
             send_middle(u)
             send_far_end(u)
-        many(spread, (1, QUERY), (2, QUERY), (3, QUERY))
-        many(spread, (1, KEY), (2, KEY))
-        many(relay, (1, QUERY), (2, QUERY), (3, QUERY))
-        many(spread, (3, KEY), (1, VALUE), (2, VALUE))
-        many(relay, (1, KEY), (2, KEY))
+        many(spread, (3, KEY), (2, VALUE), (1, QUERY))
+        many(relay, (3, QUERY), (2, KEY))
+        many(spread, (2, OUT_RET))
+        many(relay, (3, KEY), (2, VALUE))
+        many(spread, (1, KEY), (2, OUT_ATT))
+        many(relay, (1, QUERY))
         many(spread, (3, VALUE))
+        many(relay, (2, OUT_RET), (1, KEY))
+        many(spread, (1, VALUE))
         line_relay(lat_part(0), 1, 1)
-        many(relay, (3, KEY))
+        line_pair(lat_part(0), 1)
         project(QUERY)
-        many(relay, (1, VALUE), (2, VALUE))
+        many(relay, (2, OUT_ATT), (3, VALUE), (1, VALUE))
+        line_relay(lat_part(1), 2, 1)
+        line_pair(lat_part(1), 2)
         many(spread, (1, OUT_RET))
-        line_relay(lat_part(1), 2, 1)
-        many(relay, (3, VALUE))
         project(KEY)
-        many(spread, (1, OUT_ATT))
+        many(spread, (3, OUT_RET), (1, OUT_ATT))
 
     project(VALUE)
     for d in others:
@@ -989,23 +1094,31 @@
     own_state.wait()
     own_kvup.wait()
     own_qup.wait()
-    many(spread, (2, OUT_RET))
+    pl.when(is_end)(lambda: many(spread, (2, OUT_RET)))
+    pl.when(~is_end)(lambda: many(relay, (1, OUT_RET)))
     for b in range(n_sp):
         with jax.named_scope(f"retention#b={b}"):
             retention(b)
-    many(spread, (3, OUT_RET), (2, OUT_ATT))
-    pl.when(~is_end)(lambda: many(relay, (1, OUT_RET)))
-    many(relay, (2, OUT_RET))
-    many(spread, (3, OUT_ATT))
-    pl.when(~is_end)(lambda: many(relay, (1, OUT_ATT)))
+
+    @pl.when(is_end)
+    def _():
+        many(spread, (3, OUT_RET), (2, OUT_ATT))
+        many(relay, (2, OUT_RET))
+        many(spread, (3, OUT_ATT))
+
+    @pl.when(~is_end)
+    def _():
+        many(spread, (3, OUT_ATT))
+        many(relay, (3, OUT_RET), (1, OUT_ATT))
 
     blocks = n_sp // LAT_PARTS
     for i in range(LAT_PARTS):
-        line_pair(lat_part(i), i + 1)
+        pl.when(is_end)(lambda i=i: line_pair(lat_part(i), i + 1))
         if i == 0:
-            many(relay, (3, OUT_RET))
+            pl.when(is_end)(lambda: many(relay, (3, OUT_RET)))
         else:
-            many(relay, (2, OUT_ATT), (3, OUT_ATT))
+            pl.when(is_end)(lambda: many(relay, (2, OUT_ATT)))
+            many(relay, (3, OUT_ATT))
         pair_arrive(lat_part(i), i + 1, True)
         for b in range(i * blocks, (i + 1) * blocks):
             with jax.named_scope(f"expand#b={b}"):
@@ -1016,19 +1129,29 @@
     for u in out_weights:
         for k in range(n_sp):
             arrive(k, u)
-    order = (3 - 3 * upper, 2 - upper, z + 1 - 2 * (z % 2), z)
-    for step, b in enumerate(order):
+    turns = [(j, c) for j in range(n_sp) for c in range(OUT_PARTS)]
+    shared = [(j, c) for j in range(2) for c in range(OUT_PARTS)]
+    for step, turn in enumerate(turns):
         with jax.named_scope(f"out#b={step}"):
-            project_out(b)
+            project_out(*turn)
         if step:
-            send_rows(order[step - 1])
-    send_rows(order[-1])
-    total = own_sum[z]
-    for k in others:
-        with jax.named_scope(f"rows#k={k}"):
-            row_copy(0, origin_of(k)).wait_recv()
-        total = total + row_in[origin_of(k)].astype(f32)
-    out_ref[...] = total.astype(bf16)
+            finish_out(*turns[step - 1])
+        if step >= LEAD and step - LEAD < len(shared):
+            pl.when(~is_end)(lambda step=step: combine(*shared[step - LEAD]))
+    finish_out(*turns[-1])
+
+    @pl.when(~is_end)
+    def _():
+        for turn in shared[len(turns) - LEAD :]:
+            combine(*turn)
+
+    for c in range(OUT_PARTS):
+        total = own_sum[n_sp - 1, :, out_columns(c)]
+        for k in range(2):
+            with jax.named_scope(f"rows#k={k}"):
+                rows_arrival(k, c).wait_recv()
+            total = total + row_in[k, c].astype(f32)
+        out_ref[:, out_columns(c)] = total.astype(bf16)
 
     for u in range(UNITS):
         for k in range(n_sp):
@@ -1050,9 +1173,11 @@
     line_drain(tok_part, 0, False)
     for i in range(LAT_PARTS):
         line_drain(lat_part(i), i + 1, True)
-    for b in range(n_sp):
-        out_copy(b).wait_send()
-        pl.when(z != b)(lambda b=b: row_copy(b, z).wait_send())
+    for j in range(n_sp):
+        for c in range(OUT_PARTS):
+            pair_sum(j, c).wait_send()
+            if j < n_sp - 1:
+                near_rows(j, c).wait_send()
 
 
 def heads_plan(
@@ -1087,6 +1212,19 @@
     rope_cos, rope_sin = wave_tables(length, ROPE_DIM)
     pair_cos = np.concatenate([rope_cos] * 4, axis=1)
     pair_sin = np.concatenate([-rope_sin, rope_sin] * 2, axis=1)
+    small = (
+        w_rope_key.T,
+        head_rate[None],
+        norm_gain[None],
+        q_lat_gain,
+        kv_lat_gain[None],
+        att_norm_gain.reshape(n_sp, 1, -1),
+        ret_norm_gain.reshape(n_sp, 1, -1),
+        ret_cos,
+        ret_sin,
+        pair_cos,
+        pair_sin,
+    )
     dma = pltpu.SemaphoreType.DMA
     vmem = pltpu.VMEM
     f32, bf16 = jnp.float32, jnp.bfloat16
@@ -1097,13 +1235,14 @@
     mixed = pl.pallas_call(
         functools.partial(layer_kernel, n_sp, q_wide, kv_wide),
         out_shape=jax.ShapeDtypeStruct((half, out_wide), bf16),
-        in_specs=[any_spec] * 8 + [vmem_spec, any_spec] + [vmem_spec] * 10 + [any_spec] * 3,
+        in_specs=[any_spec] * 23,
         out_specs=vmem_spec,
         scratch_shapes=[
             vmem((n_sp, rows, width), bf16),
             vmem((n_sp * 4 * w_rows, (UNITS - 1) * WIDE), bf16),
             vmem((n_sp * 4 * w_rows, q_wide), bf16),
             vmem((w_rows, q_wide), bf16),
+            *[vmem(x.shape, x.dtype) for x in small],
             vmem((n_sp,) + decay_shift.shape[1:], f32),
             vmem((length, width), bf16),
             vmem((length, WIDE), f32),
@@ -1121,13 +1260,14 @@
             vmem((w_q_up.shape[0], att_heads * (NOPE_DIM + ROPE_DIM)), bf16),
             vmem((length, WIDE + att_heads * VAL_DIM), bf16),
             vmem((n_sp, half, out_wide), f32),
-            vmem((n_sp, half, out_wide), bf16),
-            vmem((n_sp, half, out_wide), bf16),
-            vmem((n_sp, half, out_wide), bf16),
-            vmem((n_sp, half, out_wide), bf16),
+            *[vmem((n_sp, OUT_PARTS, half, out_wide // OUT_PARTS), bf16)] * 2,
+            vmem((n_sp - 1, OUT_PARTS, half, out_wide // OUT_PARTS), bf16),
+            *[vmem((2, OUT_PARTS, half, out_wide // OUT_PARTS), bf16)] * 2,
             dma((12,)),
             *[dma((n_sp, UNITS))] * 8,
-            *[dma((3, n_sp))] * 2,
+            *[dma((1, n_sp))] * 2,
+            dma((len(small),)),
+            *[dma((n_sp, OUT_PARTS))] * 5,
             *[dma((LAT_PARTS + 1, n_sp))] * 5,
         ],
         compiler_params=pltpu.CompilerParams(
@@ -1142,18 +1282,9 @@
         w_ret_value,
         w_ret_out,
         w_att_out,
-        w_rope_key,
+        small[0],
         decay_shift[0],
-        head_rate[None],
-        norm_gain[None],
-        q_lat_gain[None],
-        kv_lat_gain[None],
-        att_norm_gain.reshape(n_sp, 1, -1),
-        ret_norm_gain.reshape(n_sp, 1, -1),
-        ret_cos,
-        ret_sin,
-        pair_cos,
-        pair_sin,
+        *small[1:],
         w_q_up,
         w_kv_up,
         start_state[0],

time: 104 us -> 93.2 us (0.90)
  Pallas kernels: 99.4 us -> 90.6 us
  local copies, waits for them, and re-layouts: 4.37 us -> 1.67 us
    pallas_call x1, Pallas kernels: 99.4 us -> 90.6 us  [heads_plan(): pl.pallas_call(functools.partial(layer_kernel, n_sp, q_wide, kv_wide), ou...]
    unnamed x2 -> x1, local copies, waits for them, and re-layouts: 3.1 us -> 1.67 us
    broadcast_in_dim x1 -> x0, local copies, waits for them, and re-layouts: 1.26 us -> none  [heads_plan(): q_lat_gain[None]]
where the time goes in v3:
time: 93.2 us; the launch traced here: 92.3 us
  Pallas kernels  90.6 us (97%)
  local copies, waits for them, and re-layouts  1.67 us (2%)
    pallas_call x1, Pallas kernels, heads_plan(): pl.pallas_call(functools.partial(layer_kernel, n_sp, q_wide, kv_wide), ou...  90.6 us

profile of v3, /device:TPU:9, one launch (start us, length us, event | category | flops | bytes accessed | tf_op | source)
XLA Modules:
  0.0 92.3 jit_solution(1251732421508722856)
XLA Ops:
  0.0 90.6 %shard_map.217 = bf16[64,2048]{1,0:T(8,128)(2,1)} custom-call(bf16[128,2048]{1,0:T(8,128)(2,1)} %bitcast.12, bf16[128,384]{1,0:T(8,128)(2,1)} %wqd_ref.1, bf16[128,256]{1,0:T(8,128)(2,1)} %wkvd_ref.1, bf16[128,1024]{1,0:T(8,128)(2,1)} %wq_ref.1, bf16[128,1024]{1,0:T(8,128)(2,1)} %wk_ref.1, bf16[128,1024]{1,0:T(8,128)(2,1)} %wv_ref.1, ...), custom_call_target="tpu_custom_call" | custom-call | tf_op jit(solution)/shard_map/pallas_call | solution.py:1235
  90.6 1.7 %copy.25 = bf16[1,64,2048]{2,1,0:T(8,128)(2,1)} copy(bf16[1,64,2048]{2,1,0:T(8,128)(2,1)} %bitcast.11) | data formatting | bytes 524288

commit v4 on v3

--- a/solution.py
+++ b/solution.py
@@ -284,11 +284,10 @@
 MESH = pl.DeviceIdType.MESH
 WIDE = RET_DIM
 CONTRACT = (((1,), (1,)), ((), ()))
-UNITS = 6
-LAT, QUERY, KEY, VALUE, OUT_RET, OUT_ATT = range(UNITS)
+UNITS = 7
+LAT, QUERY, KEY, VALUE, OUT_RET, OUT_ATT, OUT_ATT2 = range(UNITS)
 LAT_PARTS = 2
 OUT_PARTS = 2
-LEAD = 5
 
 
 def heads_fit(mesh, ret_local, sequences, q_wide, kv_wide, up_wide):
@@ -418,9 +417,11 @@
     rows = tok_ref.shape[0]
     length = n_sp * rows
     half = rows // 2
-    weights = (None, wq_ref, wk_ref, wv_ref, wr_ref, wa_ref)
+    weights = (None, wq_ref, wk_ref, wv_ref, wr_ref, wa_ref, wa_ref)
     f32, bf16 = jnp.float32, jnp.bfloat16
-    q_place, kv_place = n_sp // 2 - 1, n_sp // 2
+    q_place, kv_place = 0, n_sp - 1
+    att_first = n_sp // 2 - 1
+    middles = (att_first, att_first + 1)
     others = range(1, n_sp)
 
     def remote(src, dst, send, recv, **where):
@@ -457,7 +458,8 @@
 
 
     def piece(u, dest):
-        return weights[u].at[:, at(dest, WIDE)]
+        column = dest if u < OUT_ATT else 2 * (dest - att_first) + u - OUT_ATT
+        return weights[u].at[:, at(column, WIDE)]
 
     def part(owner_z, owner_f, u):
         where = at(owner_z * fs + owner_f)
@@ -466,7 +468,8 @@
         return w_all.at[where, (u - 1) * WIDE : u * WIDE]
 
     def has(u, place):
-        return (place == q_place) | (place == kv_place) if u == LAT else True
+        edge = (place == q_place) | (place == kv_place)
+        return edge if u == LAT else ~edge if u >= OUT_ATT else True
 
     def when(condition, action):
         if condition is True:
@@ -508,9 +511,9 @@
     def own_lat_copy(place):
         return pltpu.make_async_copy(lat_sources[place], part(z, f, LAT), local_sem.at[LAT])
 
-    def send(u):
-        for k in others:
-            z_copy(origin_of(k), u).start()
+    def send(u, *to):
+        for k in to or others:
+            when(has(u, origin_of(k)), lambda k=k: z_copy(origin_of(k), u).start())
 
     def send_lat(place):
         pl.when(z != place)(lambda: z_copy(place, LAT, lat_sources[place]).start())
@@ -554,16 +557,7 @@
     lat_rows = length // LAT_PARTS
 
     def lat_part(i):
-        return lambda origin: lat_all.at[t, origin - q_place, pl.ds(i * lat_rows, lat_rows)]
-
-    def sends(row, origin):
-        return True if row == 0 else has(LAT, origin)
-
-    def both(condition, more):
-        return condition if more is True else condition & more
-
-    def steps(row):
-        return range(1, n_sp - 1 if row == 0 else 2)
+        return lambda origin: lat_all.at[t, origin // (n_sp - 1), pl.ds(i * lat_rows, lat_rows)]
 
     def line_copy(where, row, dest, src=None):
         return remote(
@@ -590,7 +584,7 @@
         for distance in distances:
             for dest in range(n_sp):
                 condition = direct(dest) & ((z - dest == distance) | (dest - z == distance))
-                pl.when(both(condition, sends(row, z)))(
+                pl.when(condition)(
                     lambda dest=dest: line_copy(where, row, dest, src).start()
                 )
 
@@ -600,7 +594,7 @@
         for middle, dest in ends:
             origin = middle + (middle - dest) * distance
 
-            @pl.when(both(z == middle, sends(row, origin)))
+            @pl.when(z == middle)
             def _(origin=origin, dest=dest):
                 with jax.named_scope(f"line#r={row}#k={distance}"):
                     relay_copy(where, row, origin, dest).wait_recv()
@@ -614,7 +608,7 @@
             for origin in range(n_sp):
                 here = (z - origin == distance) | (origin - z == distance)
 
-                @pl.when(both(here, sends(row, origin)))
+                @pl.when(here)
                 def _(origin=origin):
                     with jax.named_scope(f"pass#r={row}#k={distance}"):
                         pl.when(~was_relayed(origin))(
@@ -622,34 +616,54 @@
                         )
                     pair_copy(where, row, origin).start()
 
-    def pair_own(where, row):
-        for origin in range(n_sp):
-            pl.when(both(origin == z, sends(row, origin)))(
-                lambda origin=origin: pair_copy(where, row, origin).start()
-            )
-
-    def pair_arrive(where, row, own):
+    def pair_arrive(where, row):
         with jax.named_scope(f"pair#r={row}"):
             for origin in range(n_sp):
-                condition = sends(row, origin) if own else both(origin != z, sends(row, origin))
-                when(condition, lambda origin=origin: pair_copy(where, row, origin).wait_recv())
-
-    def line_drain(where, row, own):
+                pl.when(origin != z)(
+                    lambda origin=origin: pair_copy(where, row, origin).wait_recv()
+                )
+
+    def line_drain(where, row):
         for dest in range(n_sp):
-            pl.when(both(direct(dest), sends(row, z)))(
-                lambda dest=dest: line_copy(where, row, dest).wait_send()
-            )
+            pl.when(direct(dest))(lambda dest=dest: line_copy(where, row, dest).wait_send())
         for middle, dest in ends:
-            for distance in steps(row):
+            for distance in range(1, n_sp - 1):
                 origin = middle + (middle - dest) * distance
-                pl.when(both(z == middle, sends(row, origin)))(
+                pl.when(z == middle)(
                     lambda origin=origin, dest=dest: relay_copy(
                         where, row, origin, dest
                     ).wait_send()
                 )
         for origin in range(n_sp):
-            condition = sends(row, origin) if own else both(origin != z, sends(row, origin))
-            when(condition, lambda origin=origin: pair_copy(where, row, origin).wait_send())
+            pl.when(origin != z)(
+                lambda origin=origin: pair_copy(where, row, origin).wait_send()
+            )
+
+
+    near_end, far_end = upper * (n_sp - 1), (1 - upper) * (n_sp - 1)
+
+    def lat_copy(i, origin, to):
+        ref = lat_part(i)(origin)
+        return remote(ref, ref, l_send.at[i + 1, 0], l_recv.at[i + 1, origin], sp=to)
+
+    def lat_send(i):
+        return lat_copy(i, z, z + 1 - 2 * upper)
+
+    def lat_forward(i):
+        with jax.named_scope(f"latnear#i={i}"):
+            lat_copy(i, near_end, z).wait_recv()
+        lat_copy(i, near_end, n_sp - 1 - z).start()
+        pair_copy(lat_part(i), i + 1, near_end).start()
+
+    def lat_far(i):
+        with jax.named_scope(f"latfar#i={i}"):
+            lat_copy(i, far_end, z).wait_recv()
+        pair_copy(lat_part(i), i + 1, far_end).start()
+
+    def lat_arrive(i):
+        with jax.named_scope(f"latpair#i={i}"):
+            for origin in (q_place, kv_place):
+                pair_copy(lat_part(i), i + 1, origin).wait_recv()
 
     def shift_copy(d):
         to = (z + d) % n_sp
@@ -683,19 +697,23 @@
             copy.start()
         own_tok.start()
         own_shift.start()
-        own_kvup.start()
-        own_qup.start()
+
+        @pl.when(~is_end)
+        def _():
+            own_kvup.start()
+            own_qup.start()
+
         own_state.start()
         for d in others:
             shift_copy(d).start()
 
-    own_tok = pltpu.make_async_copy(tok_ref, tok_all.at[z], local_sem.at[6])
-    own_shift = pltpu.make_async_copy(shift_ref, shift_all.at[z], local_sem.at[7])
+    own_tok = pltpu.make_async_copy(tok_ref, tok_all.at[z], local_sem.at[12])
+    own_shift = pltpu.make_async_copy(shift_ref, shift_all.at[z], local_sem.at[13])
     att_wide = kvup.shape[1]
-    own_kvup = pltpu.make_async_copy(kvup_ref.at[:, at(z, att_wide)], kvup, local_sem.at[8])
+    own_kvup = pltpu.make_async_copy(kvup_ref.at[:, at(z - att_first, att_wide)], kvup, local_sem.at[8])
     own_state = pltpu.make_async_copy(start_ref.at[z], state, local_sem.at[9])
     up_wide = qup.shape[1]
-    own_qup = pltpu.make_async_copy(qup_ref.at[:, at(z, up_wide)], qup, local_sem.at[10])
+    own_qup = pltpu.make_async_copy(qup_ref.at[:, at(z - att_first, up_wide)], qup, local_sem.at[10])
     own_kvd = pltpu.make_async_copy(wkvd_ref, kv_src.at[:, :kv_wide], local_sem.at[11])
 
     def norm_block(i):
@@ -732,12 +750,12 @@
 
     def finish_lat():
         def block(i, carry):
-            lat_all[t, z - q_place, at(i), :kv_wide] = acc_lat[at(i), :kv_wide].astype(bf16)
+            lat_all[t, upper, at(i), :kv_wide] = acc_lat[at(i), :kv_wide].astype(bf16)
             pair = acc_lat[at(i), kv_wide:]
             turned = pair * pcos_ref[at(i), :] + pltpu.roll(pair, ROPE_DIM, 1) * psin_ref[at(i), :]
             lane = lax.broadcasted_iota(jnp.int32, turned.shape, 1)
             turned = jnp.where(lane < ROPE_DIM, turned, pltpu.roll(turned, ROPE_DIM, 1))
-            lat_all[t, z - q_place, at(i), kv_wide:] = jnp.where(
+            lat_all[t, upper, at(i), kv_wide:] = jnp.where(
                 z == kv_place, turned, pair
             ).astype(bf16)
             return carry
@@ -811,21 +829,26 @@
             return (scaled * gain[...].reshape(1, wide * 2)).astype(bf16)
 
         query = jnp.dot(latent(0, q_wide, qgain_ref), qup[...], preferred_element_type=f32)
-        first, middle, end = query[:, :128], query[:, 128:256], query[:, 256:]
-        lane = lax.broadcasted_iota(jnp.int32, first.shape, 1)
-        second = jnp.where(
-            lane < ROPE_DIM, pltpu.roll(middle, ROPE_DIM, 1), pltpu.roll(end, ROPE_DIM, 1)
-        )
-        pair = jnp.where(lane < ROPE_DIM, middle, end)
-        quarter = ROPE_DIM // 2
-        swapped = jnp.where(
-            lane % ROPE_DIM < quarter,
-            pltpu.roll(pair, 2 * ROPE_DIM - quarter, 1),
-            pltpu.roll(pair, quarter, 1),
-        )
-        qn[at(i), :NOPE_DIM] = first.astype(bf16)
-        qn[at(i), NOPE_DIM:] = second.astype(bf16)
-        qr[at(i), :] = (pair * pcos_ref[at(i), :] + swapped * psin_ref[at(i), :]).astype(bf16)
+        for pair_at in range(att_heads // 2):
+            lanes = query[:, pair_at * 384 : (pair_at + 1) * 384]
+            first, middle, end = lanes[:, :128], lanes[:, 128:256], lanes[:, 256:]
+            lane = lax.broadcasted_iota(jnp.int32, first.shape, 1)
+            second = jnp.where(
+                lane < ROPE_DIM, pltpu.roll(middle, ROPE_DIM, 1), pltpu.roll(end, ROPE_DIM, 1)
+            )
+            pair = jnp.where(lane < ROPE_DIM, middle, end)
+            quarter = ROPE_DIM // 2
+            swapped = jnp.where(
+                lane % ROPE_DIM < quarter,
+                pltpu.roll(pair, 2 * ROPE_DIM - quarter, 1),
+                pltpu.roll(pair, quarter, 1),
+            )
+            base = 2 * pair_at * NOPE_DIM
+            qn[at(i), base : base + NOPE_DIM] = first.astype(bf16)
+            qn[at(i), base + NOPE_DIM : base + 2 * NOPE_DIM] = second.astype(bf16)
+            qr[at(i), pair_at * 128 : (pair_at + 1) * 128] = (
+                pair * pcos_ref[at(i), :] + swapped * psin_ref[at(i), :]
+            ).astype(bf16)
         expanded[at(i), :] = jnp.dot(
             latent(1, kv_wide, kvgain_ref), kvup[...], preferred_element_type=f32
         ).astype(bf16)
@@ -840,9 +863,9 @@
         k_at = lax.broadcasted_iota(jnp.int32, (rows, seen), 1)
         for h in range(att_heads):
             base = h * (NOPE_DIM + VAL_DIM)
-            turned = qr[block, :]
+            turned = qr[block, h // 2 * 128 : (h // 2 + 1) * 128]
             lane = lax.broadcasted_iota(jnp.int32, turned.shape, 1)
-            turned = jnp.where(lane // ROPE_DIM == h, turned, jnp.zeros_like(turned))
+            turned = jnp.where(lane // ROPE_DIM == h % 2, turned, jnp.zeros_like(turned))
             s = lax.dot_general(
                 qn[block, h * NOPE_DIM : (h + 1) * NOPE_DIM],
                 expanded[:seen, base : base + NOPE_DIM],
@@ -859,7 +882,7 @@
                 preferred_element_type=f32,
             ) / jnp.sum(p, axis=-1, keepdims=True)
             scaled = raw * lax.rsqrt(jnp.mean(raw * raw, axis=-1, keepdims=True) + EPSILON)
-            gain = again_ref[z][:, h * VAL_DIM : (h + 1) * VAL_DIM]
+            gain = again_ref[z - att_first][:, h * VAL_DIM : (h + 1) * VAL_DIM]
             merged[block, WIDE + h * VAL_DIM : WIDE + (h + 1) * VAL_DIM] = (
                 scaled * gain
             ).astype(bf16)
@@ -869,7 +892,7 @@
 
     def out_place(j):
         depth_in = z + upper * (n_sp - 1 - 2 * z)
-        found = (depth_in * 0 + 3, depth_in * 0 + 2, 1 - depth_in, depth_in)[j]
+        found = (3 - 3 * depth_in, 2 + depth_in, 1 + depth_in, depth_in)[j]
         return found + upper * (n_sp - 1 - 2 * found)
 
     def out_columns(c):
@@ -888,9 +911,9 @@
     def far_rows(j, c):
         return remote(
             row_out.at[j, c],
-            far_in.at[j, c],
+            far_in.at[j % 2, c],
             r_send.at[j, c],
-            far_recv.at[j, c],
+            far_recv.at[j % 2, c],
             sp=z + 1 - 2 * upper,
         )
 
@@ -903,41 +926,42 @@
         return remote(row_in.at[k, c], row_in.at[k, c], r_send.at[0, c], r_recv.at[k, c], tp=other)
 
     def project_out(j, c):
-        first = slice(c * part_wide, (c + 1) * part_wide)
-        got = lax.dot_general(
-            merged[at(out_place(j)), :],
-            w_all[first, (OUT_RET - 1) * WIDE :],
-            CONTRACT,
-            preferred_element_type=f32,
-        )
-        front, back = got[:half, :], got[half:, :]
-        pair_out[j, c] = jnp.where(t == 0, back, front).astype(bf16)
-        pair_sum(j, c).start()
-        own_sum[j, :, out_columns(c)] = jnp.where(t == 0, front, back)
+        def action(wide):
+            start = (OUT_RET - 1) * WIDE
+            got = lax.dot_general(
+                merged[at(out_place(j)), :wide],
+                w_all[out_columns(c), start : start + wide],
+                CONTRACT,
+                preferred_element_type=f32,
+            )
+            front, back = got[:half, :], got[half:, :]
+            pair_out[j, c] = jnp.where(t == 0, back, front).astype(bf16)
+            pair_sum(j, c).start()
+            own_sum[j, :, out_columns(c)] = jnp.where(t == 0, front, back)
+
+        pl.when(is_end)(lambda: action(WIDE))
+        pl.when(~is_end)(lambda: action(merged.shape[1]))
 
     def finish_out(j, c):
         with jax.named_scope("rows_pair"):
             pair_sum(j, c).wait_recv()
         total = own_sum[j, :, out_columns(c)] + pair_in[j, c].astype(f32)
-        own_sum[j, :, out_columns(c)] = total
         if j == n_sp - 1:
+            own_sum[j, :, out_columns(c)] = total
             return
 
         def ship(copy):
             row_out[j, c] = total.astype(bf16)
             copy.start()
 
-        if j == n_sp - 2:
-            ship(near_rows(j, c))
-        else:
-            pl.when(is_end)(lambda: ship(far_rows(j, c)))
-
-    def combine(j, c):
-        with jax.named_scope("combine"):
-            far_rows(j, c).wait_recv()
-        total = own_sum[j, :, out_columns(c)] + far_in[j, c].astype(f32)
-        row_out[j, c] = total.astype(bf16)
-        sum_rows(j, c).start()
+        def combine():
+            with jax.named_scope("combine"):
+                far_rows(j - 1, c).wait_recv()
+            row_out[j, c] = (total + far_in[j - 1, c].astype(f32)).astype(bf16)
+            sum_rows(j, c).start()
+
+        pl.when(is_end)(lambda: ship((near_rows if j == n_sp - 2 else far_rows)(j, c)))
+        pl.when(~is_end)(lambda: ship(near_rows(j, c)) if j == 0 else combine())
 
 
     def many(action, *pairs):
@@ -945,39 +969,38 @@
             action(k, u)
 
     def norm_others():
-        pair_arrive(tok_part, 0, False)
+        pair_arrive(tok_part, 0)
         for k in others:
             norm_block(origin_of(k))
 
-    def send_near_end(u):
-        for dest in (0, n_sp - 1):
-            pl.when(direct(dest))(lambda dest=dest: z_copy(dest, u).start())
-
-    def send_far_end(u):
-        for dest in (0, n_sp - 1):
-            pl.when((z - dest == 2) | (dest - z == 2))(lambda dest=dest: z_copy(dest, u).start())
-
-    def send_middle(u):
-        for dest in lat_sources:
-            pl.when(z != dest)(lambda dest=dest: z_copy(dest, u).start())
+    def retain():
+        for d in others:
+            shift_copy(d).wait_recv()
+        own_shift.wait()
+        own_state.wait()
+        for b in range(n_sp):
+            with jax.named_scope(f"retention#b={b}"):
+                retention(b)
+
+    def output():
+        turns = [(j, c) for j in range(n_sp) for c in range(OUT_PARTS)]
+        for step, turn in enumerate(turns):
+            with jax.named_scope(f"out#b={step}"):
+                project_out(*turn)
+            if step:
+                finish_out(*turns[step - 1])
+        finish_out(*turns[-1])
 
     ret_weights = (QUERY, KEY, VALUE)
-    out_weights = (OUT_RET, OUT_ATT)
+    out_weights = (OUT_RET, OUT_ATT, OUT_ATT2)
 
     own_kvd.start()
     for copy in small_copies:
         copy.start()
-    pl.when(~is_end)(lambda: line_start(tok_part, 0, tok_ref.at[mine]))
-
-    @pl.when(z == q_place)
-    def _():
-        own_lat_copy(q_place).start()
-
-    for u in ret_weights + out_weights:
-        own_copy(u).start()
+    pl.when(z == q_place)(lambda: own_lat_copy(q_place).start())
     send_lat(q_place)
-    for u in ret_weights + out_weights:
-        send_near_end(u)
+    for u in range(QUERY, UNITS):
+        when(has(u, z), lambda u=u: own_copy(u).start())
     with jax.named_scope("kvsrc"):
         own_kvd.wait()
         for copy in small_copies:
@@ -986,164 +1009,124 @@
     kv_src[:, kv_wide:] = jnp.concatenate(
         [rope, rope[:, ROPE_DIM // 2 :], rope[:, : ROPE_DIM // 2]], axis=1
     )
-
-    @pl.when(z == kv_place)
-    def _():
-        own_lat_copy(kv_place).start()
-
+    pl.when(z == kv_place)(lambda: own_lat_copy(kv_place).start())
     send_lat(kv_place)
 
     @pl.when(is_end)
     def _():
         line_start(tok_part, 0, tok_ref.at[mine], (2, 1))
+        for k in (1, 2):
+            for u in (*ret_weights, *out_weights):
+                send(u, k)
         for u in ret_weights:
-            send(u)
-        for u in out_weights:
-            z_copy(origin_of(1), u).start()
+            send(u, 3)
         start_inputs()
-        many(spread, (0, QUERY), (0, KEY), (0, VALUE), (0, OUT_RET), (0, OUT_ATT))
+        many(spread, (0, LAT), (0, QUERY), (0, KEY), (1, LAT), (0, VALUE))
+        many(relay, (0, LAT))
+        many(spread, (2, LAT), (3, LAT))
         own_tok.wait()
         norm_block(z)
-        many(spread, (1, QUERY), (1, KEY))
-        many(relay, (0, QUERY), (0, KEY))
-        many(spread, (1, VALUE))
-        many(relay, (0, VALUE))
-        many(spread, (1, OUT_RET), (1, OUT_ATT))
-        many(relay, (0, OUT_RET), (0, OUT_ATT))
-        many(relay, (1, QUERY), (1, KEY))
-        many(spread, (2, QUERY))
-        many(relay, (1, VALUE))
-        many(spread, (2, KEY))
-        many(relay, (1, OUT_RET), (1, OUT_ATT))
-        many(spread, (2, VALUE))
-        many(relay, (2, QUERY), (2, KEY))
-        many(spread, (3, QUERY))
-        many(relay, (2, VALUE))
-        many(spread, (3, KEY))
-        many(relay, (3, QUERY))
-        many(spread, (3, VALUE))
-        many(relay, (3, KEY))
+        many(relay, (0, QUERY), (1, LAT), (0, KEY))
+        many(spread, (0, OUT_RET))
+        many(relay, (2, LAT), (3, LAT))
+        many(spread, (1, QUERY), (1, KEY), (1, VALUE))
+        many(relay, (0, VALUE), (0, OUT_RET))
+        many(spread, (1, OUT_RET))
+        many(relay, (1, QUERY), (1, KEY), (1, VALUE), (1, OUT_RET))
         line_pair(tok_part, 0)
-        for u in out_weights:
-            z_copy(origin_of(2), u).start()
-            z_copy(origin_of(3), u).start()
         norm_others()
-        wait_tables()
-        project(QUERY)
-        many(relay, (3, VALUE))
-        project(KEY)
-
-    @pl.when(~is_end)
-    def _():
-        for u in ret_weights:
-            send_far_end(u)
-        for u in ret_weights:
-            send_middle(u)
-        start_inputs()
-        many(spread, (0, LAT), (0, QUERY), (0, KEY))
-        many(relay, (0, LAT))
-        many(spread, (2, LAT), (3, LAT), (0, VALUE))
-        own_tok.wait()
-        norm_block(z)
-        many(relay, (0, QUERY), (0, KEY), (2, LAT))
-        line_relay(tok_part, 0, 1)
-        many(spread, (1, LAT), (0, OUT_RET), (0, OUT_ATT))
-        many(relay, (3, LAT), (0, VALUE), (1, LAT))
-        many(spread, (2, QUERY))
-        line_relay(tok_part, 0, 2)
-        line_pair(tok_part, 0)
-        many(relay, (0, OUT_RET), (0, OUT_ATT))
-        many(spread, (3, QUERY), (2, KEY))
-        norm_others()
-        many(relay, (2, QUERY))
         for k in range(n_sp):
             arrive(k, LAT)
         wait_tables()
         multiply(LAT)
         finish_lat()
         for i in range(LAT_PARTS):
-            line_start(lat_part(i), i + 1)
-        for i in range(LAT_PARTS):
-            pair_own(lat_part(i), i + 1)
-        for u in out_weights:
-            send_middle(u)
-            send_far_end(u)
-        many(spread, (3, KEY), (2, VALUE), (1, QUERY))
-        many(relay, (3, QUERY), (2, KEY))
-        many(spread, (2, OUT_RET))
-        many(relay, (3, KEY), (2, VALUE))
-        many(spread, (1, KEY), (2, OUT_ATT))
-        many(relay, (1, QUERY))
-        many(spread, (3, VALUE))
-        many(relay, (2, OUT_RET), (1, KEY))
-        many(spread, (1, VALUE))
-        line_relay(lat_part(0), 1, 1)
-        line_pair(lat_part(0), 1)
+            lat_send(i).start()
+        send(OUT_RET, 3)
+        many(spread, (2, QUERY), (2, KEY), (2, VALUE), (3, QUERY))
+        many(relay, (2, QUERY), (2, KEY))
+        many(spread, (3, KEY))
+        many(relay, (2, VALUE))
+        many(spread, (3, VALUE), (2, OUT_RET))
+        many(relay, (3, QUERY), (3, KEY))
+        many(spread, (3, OUT_RET))
+        many(relay, (3, VALUE), (2, OUT_RET))
         project(QUERY)
-        many(relay, (2, OUT_ATT), (3, VALUE), (1, VALUE))
-        line_relay(lat_part(1), 2, 1)
-        line_pair(lat_part(1), 2)
-        many(spread, (1, OUT_RET))
         project(KEY)
-        many(spread, (3, OUT_RET), (1, OUT_ATT))
-
-    project(VALUE)
-    for d in others:
-        shift_copy(d).wait_recv()
-    own_shift.wait()
-    own_state.wait()
-    own_kvup.wait()
-    own_qup.wait()
-    pl.when(is_end)(lambda: many(spread, (2, OUT_RET)))
-    pl.when(~is_end)(lambda: many(relay, (1, OUT_RET)))
-    for b in range(n_sp):
-        with jax.named_scope(f"retention#b={b}"):
-            retention(b)
-
-    @pl.when(is_end)
-    def _():
-        many(spread, (3, OUT_RET), (2, OUT_ATT))
-        many(relay, (2, OUT_RET))
-        many(spread, (3, OUT_ATT))
+        many(relay, (3, OUT_RET))
+        project(VALUE)
+        with jax.named_scope("retain"):
+            retain()
+        for k in range(n_sp):
+            arrive(k, OUT_RET)
+        output()
 
     @pl.when(~is_end)
     def _():
-        many(spread, (3, OUT_ATT))
-        many(relay, (3, OUT_RET), (1, OUT_ATT))
-
-    blocks = n_sp // LAT_PARTS
-    for i in range(LAT_PARTS):
-        pl.when(is_end)(lambda i=i: line_pair(lat_part(i), i + 1))
-        if i == 0:
-            pl.when(is_end)(lambda: many(relay, (3, OUT_RET)))
-        else:
-            pl.when(is_end)(lambda: many(relay, (2, OUT_ATT)))
-            many(relay, (3, OUT_ATT))
-        pair_arrive(lat_part(i), i + 1, True)
-        for b in range(i * blocks, (i + 1) * blocks):
-            with jax.named_scope(f"expand#b={b}"):
-                expand(b)
-        for b in range(i * blocks, (i + 1) * blocks):
-            with jax.named_scope(f"attend#b={b}"):
-                attend(b)
-    for u in out_weights:
-        for k in range(n_sp):
-            arrive(k, u)
-    turns = [(j, c) for j in range(n_sp) for c in range(OUT_PARTS)]
-    shared = [(j, c) for j in range(2) for c in range(OUT_PARTS)]
-    for step, turn in enumerate(turns):
-        with jax.named_scope(f"out#b={step}"):
-            project_out(*turn)
-        if step:
-            finish_out(*turns[step - 1])
-        if step >= LEAD and step - LEAD < len(shared):
-            pl.when(~is_end)(lambda step=step: combine(*shared[step - LEAD]))
-    finish_out(*turns[-1])
-
-    @pl.when(~is_end)
-    def _():
-        for turn in shared[len(turns) - LEAD :]:
-            combine(*turn)
+        line_start(tok_part, 0, tok_ref.at[mine])
+        for u in (*ret_weights, OUT_RET):
+            send(u, 2)
+        for u in ret_weights:
+            send(u, 1)
+        start_inputs()
+        many(spread, *[(0, u) for u in range(QUERY, UNITS)])
+        own_tok.wait()
+        norm_block(z)
+        many(relay, *[(0, u) for u in range(QUERY, UNITS)])
+        line_relay(tok_part, 0, 1)
+        line_relay(tok_part, 0, 2)
+        line_pair(tok_part, 0)
+        many(spread, (2, QUERY), (2, KEY), (1, QUERY))
+        norm_others()
+        wait_tables()
+        for u in (*ret_weights, OUT_RET):
+            send(u, 3)
+        for u in out_weights:
+            send(u, 1)
+        many(relay, (2, QUERY))
+        many(spread, (2, VALUE), (3, QUERY))
+        many(relay, (2, KEY), (1, QUERY))
+        many(spread, (1, KEY), (3, KEY))
+        many(relay, (3, QUERY), (2, VALUE))
+        many(spread, (1, VALUE), (3, VALUE))
+        many(relay, (1, KEY), (3, KEY))
+        many(spread, (2, OUT_RET), (2, OUT_ATT), (2, OUT_ATT2))
+        many(relay, (1, VALUE), (3, VALUE))
+        lat_forward(0)
+        many(spread, (1, OUT_RET))
+        project(QUERY)
+        many(relay, (2, OUT_RET), (2, OUT_ATT))
+        many(spread, (1, OUT_ATT), (1, OUT_ATT2))
+        lat_forward(1)
+        many(relay, (2, OUT_ATT2))
+        project(KEY)
+        many(spread, (3, OUT_RET), (3, OUT_ATT), (3, OUT_ATT2))
+        project(VALUE)
+        retain()
+        own_kvup.wait()
+        own_qup.wait()
+        many(relay, (1, OUT_RET))
+        lat_far(0)
+        many(relay, (1, OUT_ATT), (1, OUT_ATT2))
+        blocks = n_sp // LAT_PARTS
+        for i in range(LAT_PARTS):
+            lat_arrive(i)
+            for b in range(i * blocks, (i + 1) * blocks):
+                with jax.named_scope(f"expand#b={b}"):
+                    expand(b)
+            if i == 0:
+                lat_far(1)
+            for b in range(i * blocks, (i + 1) * blocks):
+                if i == 0:
+                    many(relay, (3, OUT_RET + b))
+                with jax.named_scope(f"attend#b={b}"):
+                    attend(b)
+            if i == 0:
+                many(relay, (3, OUT_ATT2))
+        for u in out_weights:
+            for k in range(n_sp):
+                arrive(k, u)
+        output()
 
     for c in range(OUT_PARTS):
         total = own_sum[n_sp - 1, :, out_columns(c)]
@@ -1163,16 +1146,26 @@
 
             when(has(u, z), drain)
             if k and u != LAT:
-                z_copy(origin_of(k), u).wait_send()
+                when(
+                    has(u, origin_of(k)),
+                    lambda k=k, u=u: z_copy(origin_of(k), u).wait_send(),
+                )
     for place in lat_sources:
         pl.when(z != place)(
             lambda place=place: z_copy(place, LAT, lat_sources[place]).wait_send()
         )
     for d in others:
         shift_copy(d).wait_send()
-    line_drain(tok_part, 0, False)
+    line_drain(tok_part, 0)
     for i in range(LAT_PARTS):
-        line_drain(lat_part(i), i + 1, True)
+        pl.when(is_end)(lambda i=i: lat_send(i).wait_send())
+
+        @pl.when(~is_end)
+        def _(i=i):
+            lat_copy(i, near_end, n_sp - 1 - z).wait_send()
+            for origin in (q_place, kv_place):
+                pair_copy(lat_part(i), i + 1, origin).wait_send()
+
     for j in range(n_sp):
         for c in range(OUT_PARTS):
             pair_sum(j, c).wait_send()
@@ -1206,7 +1199,7 @@
     length = n_sp * rows
     q_wide, kv_wide = w_q_down.shape[1], w_kv_down.shape[1]
     w_rows = w_q_down.shape[0]
-    att_heads = w_q_up.shape[1] // (NOPE_DIM + ROPE_DIM) // n_sp
+    att_heads = w_q_up.shape[1] // (NOPE_DIM + ROPE_DIM) // 2
 
     ret_cos, ret_sin = wave_tables(length, RET_DIM)
     rope_cos, rope_sin = wave_tables(length, ROPE_DIM)
@@ -1218,7 +1211,7 @@
         norm_gain[None],
         q_lat_gain,
         kv_lat_gain[None],
-        att_norm_gain.reshape(n_sp, 1, -1),
+        att_norm_gain.reshape(2, 1, -1),
         ret_norm_gain.reshape(n_sp, 1, -1),
         ret_cos,
         ret_sin,
@@ -1263,7 +1256,7 @@
             *[vmem((n_sp, OUT_PARTS, half, out_wide // OUT_PARTS), bf16)] * 2,
             vmem((n_sp - 1, OUT_PARTS, half, out_wide // OUT_PARTS), bf16),
             *[vmem((2, OUT_PARTS, half, out_wide // OUT_PARTS), bf16)] * 2,
-            dma((12,)),
+            dma((14,)),
             *[dma((n_sp, UNITS))] * 8,
             *[dma((1, n_sp))] * 2,
             dma((len(small),)),

time: 93.2 us -> 88.7 us (0.952)
  Pallas kernels: 90.6 us -> 86.9 us
    pallas_call x1, Pallas kernels: 90.6 us -> 86.9 us  [heads_plan(): pl.pallas_call(functools.partial(layer_kernel, n_sp, q_wide, kv_wide), ou...]
where the time goes in v4:
time: 88.7 us; the launch traced here: 88.5 us
  Pallas kernels  86.9 us (98%)
  local copies, waits for them, and re-layouts  1.67 us (2%)
    pallas_call x1, Pallas kernels, heads_plan(): pl.pallas_call(functools.partial(layer_kernel, n_sp, q_wide, kv_wide), ou...  86.9 us

profile of v4, /device:TPU:9, one launch (start us, length us, event | category | flops | bytes accessed | tf_op | source)
XLA Modules:
  0.0 88.5 jit_solution(2803407690573860419)
XLA Ops:
  0.0 86.9 %shard_map.217 = bf16[64,2048]{1,0:T(8,128)(2,1)} custom-call(bf16[128,2048]{1,0:T(8,128)(2,1)} %bitcast.12, bf16[128,384]{1,0:T(8,128)(2,1)} %wqd_ref.1, bf16[128,256]{1,0:T(8,128)(2,1)} %wkvd_ref.1, bf16[128,1024]{1,0:T(8,128)(2,1)} %wq_ref.1, bf16[128,1024]{1,0:T(8,128)(2,1)} %wk_ref.1, bf16[128,1024]{1,0:T(8,128)(2,1)} %wv_ref.1, ...), custom_call_target="tpu_custom_call" | custom-call | tf_op jit(solution)/shard_map/pallas_call | solution.py:1228
  86.9 1.7 %copy.25 = bf16[1,64,2048]{2,1,0:T(8,128)(2,1)} copy(bf16[1,64,2048]{2,1,0:T(8,128)(2,1)} %bitcast.11) | data formatting | bytes 524288

commit v5 on v4

--- a/solution.py
+++ b/solution.py
@@ -386,6 +386,7 @@
     row_out,
     row_in,
     far_in,
+    out_vmem,
     local_sem,
     z_send,
     z_recv,
@@ -398,6 +399,7 @@
     m_send,
     m_recv,
     small_sem,
+    out_sem,
     o_send,
     o_recv,
     r_send,
@@ -921,6 +923,9 @@
         return remote(
             row_out.at[j, c], row_in.at[1, c], r_send.at[j, c], r_recv.at[1, c], sp=out_place(j)
         )
+
+    def out_copy(c):
+        return pltpu.make_async_copy(out_vmem.at[c], out_ref.at[:, out_columns(c)], out_sem.at[c])
 
     def rows_arrival(k, c):
         return remote(row_in.at[k, c], row_in.at[k, c], r_send.at[0, c], r_recv.at[k, c], tp=other)
@@ -1101,13 +1106,12 @@
         many(relay, (2, OUT_ATT2))
         project(KEY)
         many(spread, (3, OUT_RET), (3, OUT_ATT), (3, OUT_ATT2))
+        lat_far(0)
         project(VALUE)
         retain()
         own_kvup.wait()
         own_qup.wait()
-        many(relay, (1, OUT_RET))
-        lat_far(0)
-        many(relay, (1, OUT_ATT), (1, OUT_ATT2))
+        many(relay, (1, OUT_RET), (1, OUT_ATT), (1, OUT_ATT2))
         blocks = n_sp // LAT_PARTS
         for i in range(LAT_PARTS):
             lat_arrive(i)
@@ -1128,14 +1132,6 @@
                 arrive(k, u)
         output()
 
-    for c in range(OUT_PARTS):
-        total = own_sum[n_sp - 1, :, out_columns(c)]
-        for k in range(2):
-            with jax.named_scope(f"rows#k={k}"):
-                rows_arrival(k, c).wait_recv()
-            total = total + row_in[k, c].astype(f32)
-        out_ref[:, out_columns(c)] = total.astype(bf16)
-
     for u in range(UNITS):
         for k in range(n_sp):
 
@@ -1165,6 +1161,17 @@
             lat_copy(i, near_end, n_sp - 1 - z).wait_send()
             for origin in (q_place, kv_place):
                 pair_copy(lat_part(i), i + 1, origin).wait_send()
+
+    for c in range(OUT_PARTS):
+        total = own_sum[n_sp - 1, :, out_columns(c)]
+        for k in range(2):
+            with jax.named_scope(f"rows#k={k}"):
+                rows_arrival(k, c).wait_recv()
+            total = total + row_in[k, c].astype(f32)
+        out_vmem[c] = total.astype(bf16)
+        out_copy(c).start()
+    for c in range(OUT_PARTS):
+        out_copy(c).wait()
 
     for j in range(n_sp):
         for c in range(OUT_PARTS):
@@ -1224,12 +1231,11 @@
     half = rows // 2
     out_wide = 4 * n_sp * w_rows
     any_spec = pl.BlockSpec(memory_space=pl.ANY)
-    vmem_spec = pl.BlockSpec(memory_space=pltpu.VMEM)
     mixed = pl.pallas_call(
         functools.partial(layer_kernel, n_sp, q_wide, kv_wide),
         out_shape=jax.ShapeDtypeStruct((half, out_wide), bf16),
         in_specs=[any_spec] * 23,
-        out_specs=vmem_spec,
+        out_specs=any_spec,
         scratch_shapes=[
             vmem((n_sp, rows, width), bf16),
             vmem((n_sp * 4 * w_rows, (UNITS - 1) * WIDE), bf16),
@@ -1256,10 +1262,12 @@
             *[vmem((n_sp, OUT_PARTS, half, out_wide // OUT_PARTS), bf16)] * 2,
             vmem((n_sp - 1, OUT_PARTS, half, out_wide // OUT_PARTS), bf16),
             *[vmem((2, OUT_PARTS, half, out_wide // OUT_PARTS), bf16)] * 2,
+            vmem((OUT_PARTS, half, out_wide // OUT_PARTS), bf16),
             dma((14,)),
             *[dma((n_sp, UNITS))] * 8,
             *[dma((1, n_sp))] * 2,
             dma((len(small),)),
+            dma((OUT_PARTS,)),
             *[dma((n_sp, OUT_PARTS))] * 5,
             *[dma((LAT_PARTS + 1, n_sp))] * 5,
         ],

time: 88.7 us -> 88.5 us (level)
  no operation moved by 1% of the time
where the time goes in v5:
time: 88.5 us; the launch traced here: 88.3 us
  Pallas kernels  86.7 us (98%)
  local copies, waits for them, and re-layouts  1.67 us (2%)
    pallas_call x1, Pallas kernels, heads_plan(): pl.pallas_call(functools.partial(layer_kernel, n_sp, q_wide, kv_wide), ou...  86.7 us

profile of v5, /device:TPU:9, one launch (start us, length us, event | category | flops | bytes accessed | tf_op | source)
XLA Modules:
  0.0 88.3 jit_solution(10560968169762119693)
XLA Ops:
  0.0 86.7 %shard_map.217 = bf16[64,2048]{1,0:T(8,128)(2,1)} custom-call(bf16[128,2048]{1,0:T(8,128)(2,1)} %bitcast.12, bf16[128,384]{1,0:T(8,128)(2,1)} %wqd_ref.1, bf16[128,256]{1,0:T(8,128)(2,1)} %wkvd_ref.1, bf16[128,1024]{1,0:T(8,128)(2,1)} %wq_ref.1, bf16[128,1024]{1,0:T(8,128)(2,1)} %wk_ref.1, bf16[128,1024]{1,0:T(8,128)(2,1)} %wv_ref.1, ...), custom_call_target="tpu_custom_call" | custom-call | tf_op jit(solution)/shard_map/pallas_call | solution.py:1234
  86.7 1.7 %copy.25 = bf16[1,64,2048]{2,1,0:T(8,128)(2,1)} copy(bf16[1,64,2048]{2,1,0:T(8,128)(2,1)} %bitcast.11) | data formatting | bytes 524288
